TPU v7x, 128 devices: a whole 4x4x4 slice. The times are simulated.
128 devices in a mesh: sp: 32 (over z, y, core), tp: 4 (over x).
Axes of the slice: x: 4, y: 4, z: 4, core: 2. Of those that a mesh axis runs over, the one named last changes fastest.
Arguments:
- tokens: bfloat16 [16384, 2048], P(('sp', 'tp')), may hold values from -6 to 6
- norm_gain: float32 [2048], replicated, may hold values from 0.1 to 1.9
- query_weight: bfloat16 [2048, 1024], P(None, 'tp'), may hold values from -0.13258252 to 0.13258252
- key_weight: bfloat16 [2048, 1024], P(None, 'tp'), may hold values from -0.13258252 to 0.13258252
- value_weight: bfloat16 [2048, 1024], P(None, 'tp'), may hold values from -0.125 to 0.125
- glu_value_weight: bfloat16 [2048, 1024], P(None, 'tp'), may hold values from -0.125 to 0.125
- glu_gate_weight: bfloat16 [2048, 1024], P(None, 'tp'), may hold values from -0.125 to 0.125
- qk_gain: float32 [2, 64], replicated, may hold values from 1 to 6
- mix_lambda: float32 [8], P('tp'), may hold values from 0.3 to 0.8
- head_gain: float32 [128], replicated, may hold values from 0.1 to 1.9
- conv_kernel: float32 [31, 1024], P(None, 'tp'), may hold values from -1 to 1
- channel_gain: float32 [1024], P('tp'), may hold values from 0.1 to 1.9
- channel_shift: float32 [1024], P('tp'), may hold values from -3 to 3
- output_weight: bfloat16 [2048, 2048], replicated, may hold values from -0.125 to 0.125
Outputs:
- mixed: bfloat16 [16384, 2048], P(('sp', 'tp'))
- log_totals: float32 [2, 8, 16384], P(None, 'tp', 'sp')
All inputs are finite; a program needn't handle non-finite values.
Results may differ from a plain program's by a relative error of at most 0.035.
Values may be sent and summed in bfloat16 or wider, within the bound.
No kernel may reach another device: no remote copies, remote signals or barrier semaphores. Data moves between devices by JAX's collectives and lax.ppermute only.
A program may use at most 128 MiB of HBM per device.

v0:
```python
import math

import jax
import jax.numpy as jnp
from jax import lax
from jax.experimental import pallas as pl
from jax.experimental.pallas import tpu as pltpu
from jax.sharding import PartitionSpec as P

NZ, NY, NC = 4, 4, 2
BIG = 2.0**100
LOG2E = math.log2(math.e)
BF = jnp.bfloat16
F32 = jnp.float32


def vmem():
    return pl.BlockSpec(memory_space=pltpu.VMEM)


def smem():
    return pl.BlockSpec(memory_space=pltpu.SMEM)


def moves(target):
    out = []
    for z in range(NZ):
        for y in range(NY):
            for c in range(NC):
                t = target(z, y, c)
                if t is not None:
                    out.append(((z * NY + y) * NC + c, (t[0] * NY + t[1]) * NC + t[2]))
    return out


def reads_query(z, y, c, qz, qy):
    return (z > 0 or qy > y) if c == 0 else qz > z


def reads_keys(z, y, c, kz, ky):
    return kz < z if c == 0 else (z < NZ - 1 or ky < y)


def stepped(z, y, along_y, step):
    return (z, (y + step) % NY) if along_y else ((z + step) % NZ, y)


def send_query(value, step):
    def target(z, y, c):
        t = stepped(z, y, c == 0, step)
        return (*t, c) if reads_query(*t, c, z, y) else None

    return lax.ppermute(value, "sp", moves(target))


def return_sum(value, step):
    def target(z, y, c):
        t = stepped(z, y, c == 0, -step)
        return (*t, c) if reads_query(z, y, c, *t) else None

    return lax.ppermute(value, "sp", moves(target))


def send_keys(value, step):
    def target(z, y, c):
        t = stepped(z, y, c == 1, step)
        return (*t, c) if reads_keys(*t, c, z, y) else None

    return lax.ppermute(value, "sp", moves(target))


def to_sibling(value):
    return lax.ppermute(value, "sp", moves(lambda z, y, c: (z, y, 1 - c)))


def along_x(value, step):
    count = lax.axis_size("tp")
    return lax.ppermute(value, "tp", [(i, (i + step) % count) for i in range(count)])


def hbm():
    return pl.BlockSpec(memory_space=pl.ANY)


def prefetch_kernel(*refs):
    n = (len(refs) - 1) // 2
    copies = [
        pltpu.make_async_copy(refs[i], refs[n + i], refs[2 * n].at[i]) for i in range(n)
    ]
    for copy in copies:
        copy.start()
    for copy in copies:
        copy.wait()


def prefetch(arrays):
    return pl.pallas_call(
        prefetch_kernel,
        out_shape=tuple(jax.ShapeDtypeStruct(a.shape, a.dtype) for a in arrays),
        in_specs=[hbm()] * len(arrays),
        out_specs=(vmem(),) * len(arrays),
        scratch_shapes=[pltpu.SemaphoreType.DMA((len(arrays),))],
        compiler_params=pltpu.CompilerParams(vmem_limit_bytes=48 * 1024 * 1024),
        cost_estimate=pl.CostEstimate(flops=2000000, bytes_accessed=12000000, transcendentals=0),
        name="prefetch",
    )(*arrays)


def project_body(pos, pieces, gain, ws, qkg, cos, sin, mine, other, normed):
    x = pos[3]
    c = pos[2]
    ats = []
    row = 0
    for ref, step in pieces:
        t = ref[...].astype(F32)
        n = t.shape[0]
        ms = jnp.mean(t * t, axis=-1, keepdims=True)
        normed[row : row + n, :] = (t * lax.rsqrt(ms + 1e-06) * gain[...]).astype(BF)
        if row % 128 == 0:
            ats.append(pl.multiple_of(lax.rem(x + step, 4) * 128, 128))
        row += n
    lane = lax.broadcasted_iota(jnp.int32, (1, 256), 1)
    first = lax.rem(lane, 64) < 32
    gi = lax.broadcasted_iota(jnp.int32, (256, 256), 0) // 64
    gj = lax.broadcasted_iota(jnp.int32, (256, 256), 1) // 64
    groups = jnp.where(gi == gj, 1.0 / 64, 0.0).astype(BF)

    def table(ref):
        v = jnp.concatenate([ref[pl.ds(at, 128), :] for at in ats], axis=0)
        return jnp.concatenate([v, v], axis=1)

    cc = table(cos)
    ss = table(sin)

    def times(w):
        return jnp.dot(normed[...], w[...], preferred_element_type=F32).astype(BF).astype(F32)

    def turned(w):
        v = times(w)
        sq = v * v
        hi = sq.astype(BF)
        lo = (sq - hi.astype(F32)).astype(BF)
        ms = jnp.dot(hi, groups, preferred_element_type=F32) + jnp.dot(
            lo, groups, preferred_element_type=F32
        )
        v = v * lax.rsqrt(ms + 1e-06) * qkg[...]
        swapped = jnp.where(first, pltpu.roll(v, 256 - 32, 1), pltpu.roll(v, 32, 1))
        return v * cc + swapped * ss

    def put(row, v, flip):
        a = v[:, :128]
        b = v[:, 128:]
        for ref, val in ((mine, jnp.where(c == 0, a, b)), (other, jnp.where(c == 0, b, a))):
            for i, at in enumerate(ats):
                part = val[i * 128 : (i + 1) * 128, :]
                ref[row : row + 128, pl.ds(at, 128)] = (part.T if flip else part).astype(BF)

    wq, wk, wv, wa, wg = ws
    put(0, turned(wq) * (LOG2E / 8.0), True)
    put(128, turned(wk), False)
    put(256, times(wv), True)
    g = times(wa) * jax.nn.sigmoid(times(wg))
    put(384, g, False)


def project_first(pos, t0, t1, t2, gain, wq, wk, wv, wa, wg, qkg, cos, sin, mine, other, normed):
    project_body(
        pos, ((t0, 0), (t1, 3), (t2, 1)), gain, (wq, wk, wv, wa, wg), qkg, cos, sin,
        mine, other, normed,
    )


def project_last(
    pos, t3, t4, gain, wq, wk, wv, wa, wg, qkg, cos, sin, mine_in, other_in, mine, other, normed
):
    project_body(
        pos, ((t3, 2), (t4, 2)), gain, (wq, wk, wv, wa, wg), qkg, cos, sin,
        mine, other, normed,
    )


def project(body, rows, pos, pieces, shared, filled):
    count = 1 + len(pieces) + len(shared) + len(filled)
    start = count - len(filled)
    return pl.pallas_call(
        body,
        out_shape=(
            jax.ShapeDtypeStruct((512, 512), BF),
            jax.ShapeDtypeStruct((512, 512), BF),
        ),
        in_specs=[smem()] + [vmem()] * (count - 1),
        out_specs=(vmem(),) * 2,
        scratch_shapes=[pltpu.VMEM((rows, 2048), BF)],
        input_output_aliases={start + i: i for i in range(len(filled))},
        compiler_params=pltpu.CompilerParams(vmem_limit_bytes=14 * 1024 * 1024),
        cost_estimate=pl.CostEstimate(
            flops=5242880 * rows, bytes_accessed=8000000, transcendentals=0
        ),
    )(pos, *pieces, *shared, *filled)


def conv_kernel_body(pos, gated, halo, taps, out, ext):
    w = jnp.where(pos[2] == 0, taps[:, :128], taps[:, 128:])
    ext[0:32, :] = jnp.zeros((32, 128), F32)
    ext[1056:1072, :] = jnp.zeros((16, 128), F32)
    ext[2:32, :] = halo[...].astype(F32)
    for i in range(8):
        ext[32 + i * 128 : 160 + i * 128, :] = gated[:, i * 128 : (i + 1) * 128].astype(F32)
    for i in range(8):
        acc = jnp.zeros((128, 128), F32)
        for r in range(8):
            moved = ext[i * 128 + r : i * 128 + r + 160, :]
            for a in range(5):
                j = a * 8 + r - 2
                if 0 <= j < 31:
                    acc = acc + w[j : j + 1, :] * moved[8 * a : 8 * a + 128]
        out[i] = acc.astype(BF)


def convolve(pos, gated, halo, taps):
    return pl.pallas_call(
        conv_kernel_body,
        out_shape=jax.ShapeDtypeStruct((8, 128, 128), BF),
        in_specs=[smem()] + [vmem()] * 3,
        out_specs=vmem(),
        scratch_shapes=[pltpu.VMEM((1072, 128), F32)],
        compiler_params=pltpu.CompilerParams(vmem_limit_bytes=4 * 1024 * 1024),
        cost_estimate=pl.CostEstimate(flops=1000000000, bytes_accessed=800000, transcendentals=0),
        name="convolve",
    )(pos, gated, halo, taps)


def split3(v):
    hi = v.astype(BF).astype(F32)
    mid = (v - hi).astype(BF).astype(F32)
    return [hi, mid, v - hi - mid]


ITEMS = [(m, qt) for m in range(2) for qt in range(4)]


def chips(pos):
    z, y, c = pos[0], pos[1], pos[2]
    own = z * 4 + y
    over_y = [own] + [z * 4 + lax.rem(y + d, 4) for d in (3, 1, 2)]
    over_z = [own] + [lax.rem(z + d, 4) * 4 + y for d in (3, 1, 2)]
    queries = [jnp.where(c == 0, a, b) for a, b in zip(over_y, over_z)]
    keys = [jnp.where(c == 0, b, a) for a, b in zip(over_y, over_z)]
    return queries, keys


def load_query(ref, qz, i):
    rows = lax.broadcasted_iota(jnp.int32, (128, 1024), 0)
    q = ref[...]
    qz[2 * i] = jnp.where(rows < 64, q, jnp.zeros_like(q))
    qz[2 * i + 1] = jnp.where(rows >= 64, q, jnp.zeros_like(q))


def load_keys(ref, kscr, vscr, b):
    for i in range(8):
        kscr[b, i * 128 : (i + 1) * 128, :] = ref[0:128, i * 128 : (i + 1) * 128]
    vscr[b] = ref[128:256, :]


def list_pairs(todo, pairs, queries, keys):
    n = jnp.int32(0)
    todo[0] = 0
    for i, s, b in pairs:
        ok = keys[b] < queries[s]

        @pl.when(ok)
        def _(n=n, i=i, b=b):
            todo[n] = i * 4 + b
            todo[n + 1] = i * 4 + b

        n = n + ok.astype(jnp.int32)
    return n


def weigh(tacc, mref, r, cols, scores, masked):
    n = scores.shape[0]
    s3 = scores.reshape(n // 8, 8, 256)
    if mref is not None:
        s3 = s3 - mref[r, :, cols][None]
    p = jnp.exp2(s3).reshape(n, 256)
    if masked:
        k = lax.broadcasted_iota(jnp.int32, (256, 256), 0)
        q = lax.broadcasted_iota(jnp.int32, (256, 256), 1)
        last = jnp.where(k <= q, p[n - 256 :], 0.0)
        p = last if n == 256 else jnp.concatenate([p[: n - 256], last], axis=0)
    tacc[r, :, cols] += jnp.sum(p.reshape(n // 8, 8, 256), axis=0)
    return p.astype(BF)


def run_pairs(todo, n, qz, kscr, vscr, sbuf, pbuf, oacc, tacc, mref):
    def score(e, m, qt):
        return jnp.dot(
            kscr[e & 3],
            qz[(e >> 2) * 2 + m, :, qt * 256 : (qt + 1) * 256],
            preferred_element_type=F32,
        )

    @pl.when(n > 0)
    def _():
        sbuf[0] = score(todo[0], 0, 0)

        @pl.loop(0, n)
        def _(t):
            e = todo[t]
            later = todo[t + 1]
            for i, (m, qt) in enumerate(ITEMS):
                if i + 1 < len(ITEMS):
                    sbuf[(i + 1) % 2] = score(e, *ITEMS[i + 1])
                else:
                    sbuf[0] = score(later, 0, 0)
                cols = slice(qt * 256, (qt + 1) * 256)
                r = (e >> 2) * 2 + m
                pbuf[i % 2] = weigh(tacc, mref, r, cols, sbuf[i % 2], False)
                oacc[r, :, cols] += jnp.dot(vscr[e & 3], pbuf[i % 2], preferred_element_type=F32)


def run_diagonal(qz, kscr, vscr, sbuf, pbuf, oacc, tacc, mref):
    for i, (m, qt) in enumerate(ITEMS):
        n = (qt + 1) * 256
        cols = slice(qt * 256, n)
        sbuf[i % 2, :n, :] = jnp.dot(kscr[0, :n, :], qz[m, :, cols], preferred_element_type=F32)
        pbuf[i % 2, :n, :] = weigh(tacc, mref, m, cols, sbuf[i % 2, :n, :], True)
        oacc[m, :, cols] += jnp.dot(vscr[0, :, :n], pbuf[i % 2, :n, :], preferred_element_type=F32)


def take_tops(todo, n, own, qz, kscr, tacc, mref):
    tacc[...] = jnp.full_like(tacc, -1e30)

    def one(b, r, qt, masked):
        cols = pl.ds(pl.multiple_of(qt * 256, 256), 256)
        sc = jnp.dot(kscr[b], qz[r, :, cols], preferred_element_type=F32)
        if masked:
            k = lax.broadcasted_iota(jnp.int32, (1024, 256), 0)
            q = lax.broadcasted_iota(jnp.int32, (1024, 256), 1) + qt * 256
            sc = jnp.where(k <= q, sc, -1e30)
        tacc[r, :, cols] = jnp.maximum(tacc[r, :, cols], jnp.max(sc.reshape(128, 8, 256), axis=0))

    if own:

        @pl.loop(0, 8)
        def _(i):
            one(0, i >> 2, i & 3, True)

    @pl.loop(0, n * 8)
    def _(i):
        e = todo[i >> 3]
        one(e & 3, (e >> 2) * 2 + ((i >> 2) & 1), i & 3, False)

    for r in range(mref.shape[0]):
        mref[r] = jnp.broadcast_to(jnp.max(tacc[r], axis=0, keepdims=True), (8, 1024))


def finish(sources, fast, pos, qz, kvs, kscr, vscr, sbuf, pbuf, oacc, tacc, mref, todo, flag):
    queries, keys = chips(pos)
    mref[...] = jnp.zeros_like(mref)
    flag[0] = 1

    @pl.loop(0, 2)
    def _(attempt):
        @pl.when(flag[0] == 1)
        def _():
            flag[1] = list_pairs(todo, fast, queries, keys)

            @pl.when(attempt == 1)
            def _():
                for b in range(4):
                    load_keys(kvs[b], kscr, vscr, b)
                every = [(i, s, b) for i, s in enumerate(sources) for b in range(4)]
                flag[1] = list_pairs(todo, every, queries, keys)
                take_tops(todo, flag[1], 0 in sources, qz, kscr, tacc, mref)
                oacc[...] = jnp.zeros_like(oacc)
                tacc[...] = jnp.zeros_like(tacc)
                if 0 in sources:
                    run_diagonal(qz, kscr, vscr, sbuf, pbuf, oacc, tacc, mref)

            run_pairs(todo, flag[1], qz, kscr, vscr, sbuf, pbuf, oacc, tacc, mref)
            worst = jnp.zeros((1, 1024), F32)
            for i, s in enumerate(sources):
                has = s == 0
                for b in range(4):
                    has = jnp.logical_or(has, keys[b] < queries[s])
                least = jnp.where(has, 1.0 / BIG, -1.0)
                for m in range(2):
                    t = jnp.sum(tacc[2 * i + m], axis=0, keepdims=True)
                    good = jnp.logical_and(t < BIG, t > least)
                    worst = jnp.where(good, worst, 1.0)
            bad = (jnp.max(worst) > 0.5).astype(jnp.int32)
            flag[0] = jnp.where(attempt == 0, bad, 0)


def write_sum(ref, i, oacc, tacc, mref):
    r = 2 * i
    t = [jnp.sum(tacc[r + m], axis=0, keepdims=True) for m in range(2)]
    ref[0:128, :] = oacc[r].astype(BF)
    ref[128:256, :] = oacc[r + 1].astype(BF)
    extra = split3(t[0]) + split3(t[1])
    extra = extra + split3(mref[r, 0:1, :]) + split3(mref[r + 1, 0:1, :])
    ref[256:272, :] = jnp.concatenate(extra + [jnp.zeros((4, 1024), F32)], axis=0).astype(BF)


def near_kernel(pos, q0, q1, q2, kv0, kv1, kv2, oacc, tacc, qz, kscr, vscr, sbuf, pbuf, todo):
    queries, keys = chips(pos)
    for i, ref in enumerate((q0, q1, q2)):
        load_query(ref, qz, i)
    for b, ref in enumerate((kv0, kv1, kv2)):
        load_keys(ref, kscr, vscr, b)
    oacc[...] = jnp.zeros_like(oacc)
    tacc[...] = jnp.zeros_like(tacc)
    n = list_pairs(todo, [(s, s, b) for b in range(3) for s in range(3)], queries, keys)
    run_diagonal(qz, kscr, vscr, sbuf, pbuf, oacc, tacc, None)
    run_pairs(todo, n, qz, kscr, vscr, sbuf, pbuf, oacc, tacc, None)


def far_kernel(
    pos, q3, kv0, kv1, kv2, kv3, near, out, token, qz, kscr, vscr, sbuf, pbuf, oacc, tacc, mref, todo, flag
):
    load_query(q3, qz, 0)
    kvs = (kv0, kv1, kv2, kv3)
    for b in range(4):
        load_keys(kvs[b], kscr, vscr, b)
    oacc[...] = jnp.zeros_like(oacc)
    tacc[...] = jnp.zeros_like(tacc)
    fast = [(0, 3, b) for b in range(4)]
    finish((3,), fast, pos, qz, kvs, kscr, vscr, sbuf, pbuf, oacc, tacc, mref, todo, flag)
    write_sum(out, 0, oacc, tacc, mref)
    token[...] = jnp.zeros_like(token)


def last_kernel(
    pos, q0, q1, q2, kv0, kv1, kv2, kv3, oin, tin, token, oacc, tacc, out1, out2, stats,
    qz, kscr, vscr, sbuf, pbuf, mref, todo, flag,
):
    for i, ref in enumerate((q0, q1, q2)):
        load_query(ref, qz, i)
    kvs = (kv0, kv1, kv2, kv3)
    load_keys(kv3, kscr, vscr, 3)
    fast = [(s, s, 3) for s in range(3)]
    finish((0, 1, 2), fast, pos, qz, kvs, kscr, vscr, sbuf, pbuf, oacc, tacc, mref, todo, flag)
    write_sum(out1, 1, oacc, tacc, mref)
    write_sum(out2, 2, oacc, tacc, mref)
    t = [jnp.sum(tacc[m], axis=0, keepdims=True) for m in range(2)]
    stats[...] = jnp.concatenate(
        t + [mref[0, 0:1, :], mref[1, 0:1, :], jnp.zeros((4, 1024), F32)], axis=0
    )


def scratch(queries, blocks, extra):
    return [
        pltpu.VMEM((2 * queries, 128, 1024), BF),
        pltpu.VMEM((blocks, 1024, 128), BF),
        pltpu.VMEM((blocks, 128, 1024), BF),
        pltpu.VMEM((2, 1024, 256), F32),
        pltpu.VMEM((2, 1024, 256), BF),
        *extra,
        pltpu.SMEM((20,), jnp.int32),
    ]


def attention_call(body, ins, outs, scratches, pairs, aliases=None):
    return pl.pallas_call(
        body,
        out_shape=outs,
        in_specs=[smem()] + [vmem()] * (len(ins) - 1),
        out_specs=(vmem(),) * len(outs),
        scratch_shapes=scratches,
        input_output_aliases=aliases or {},
        compiler_params=pltpu.CompilerParams(vmem_limit_bytes=12 * 1024 * 1024),
        cost_estimate=pl.CostEstimate(
            flops=800000000 * pairs, bytes_accessed=4000000, transcendentals=2000000 * pairs
        ),
    )(*ins)


def attend_near(pos, qs, kvs):
    outs = (
        jax.ShapeDtypeStruct((6, 128, 1024), F32),
        jax.ShapeDtypeStruct((6, 8, 1024), F32),
    )
    ins = (pos, *qs, *kvs)
    return attention_call(near_kernel, ins, outs, scratch(3, 3, []), 8)


def attend_far(pos, q, kvs, near):
    outs = (jax.ShapeDtypeStruct((272, 1024), BF), jax.ShapeDtypeStruct((8, 128), F32))
    extra = [
        pltpu.VMEM((2, 128, 1024), F32),
        pltpu.VMEM((2, 8, 1024), F32),
        pltpu.VMEM((2, 8, 1024), F32),
    ]
    return attention_call(
        far_kernel,
        (pos, q, *kvs, near),
        outs,
        scratch(1, 4, extra) + [pltpu.SMEM((2,), jnp.int32)],
        4,
    )


def attend_last(pos, qs, kvs, oacc, tacc, token):
    sent = jax.ShapeDtypeStruct((272, 1024), BF)
    outs = (
        jax.ShapeDtypeStruct((6, 128, 1024), F32),
        jax.ShapeDtypeStruct((6, 8, 1024), F32),
        sent,
        sent,
        jax.ShapeDtypeStruct((8, 1024), F32),
    )
    ins = (pos, *qs, *kvs, oacc, tacc, token)
    extra = [pltpu.VMEM((6, 8, 1024), F32)]
    return attention_call(
        last_kernel,
        ins,
        outs,
        scratch(3, 4, extra) + [pltpu.SMEM((2,), jnp.int32)],
        3,
        {8: 0, 9: 1},
    )


def merge_kernel(pos, lam, own, stats, r1, r2, r3, gain, conv, scale, shift, packed, lmine, lother):
    c = pos[2]
    mix = jnp.where(c == 0, lam[0], lam[1])

    def joined(ref, row):
        part = ref[256:272, :].astype(F32)
        return part[row : row + 1] + part[row + 1 : row + 2] + part[row + 2 : row + 3]

    heads = []
    logs = []
    for m in range(2):
        ts = [stats[m : m + 1, :]] + [joined(r, 3 * m) for r in (r1, r2, r3)]
        ms = [stats[2 + m : 3 + m, :]] + [joined(r, 6 + 3 * m) for r in (r1, r2, r3)]
        ms = [jnp.where(t > 0, v, -1e30) for t, v in zip(ts, ms)]
        top = jnp.maximum(jnp.maximum(ms[0], ms[1]), jnp.maximum(ms[2], ms[3]))
        ws = [jnp.exp2(v - top) for v in ms]
        total = ws[0] * ts[0] + ws[1] * ts[1] + ws[2] * ts[2] + ws[3] * ts[3]
        inv = 1.0 / total
        acc = own[m] * (ws[0] * inv)
        for w, r in zip(ws[1:], (r1, r2, r3)):
            acc = acc + r[m * 128 : (m + 1) * 128, :].astype(F32) * (w * inv)
        heads.append(acc)
        logs.append(top * math.log(2.0) + jnp.log(total))
    h = heads[0] - mix * heads[1]
    h = h * lax.rsqrt(jnp.mean(h * h, axis=0, keepdims=True) + 1e-06)
    lt = jnp.concatenate(logs, axis=0)
    sc = jnp.where(c == 0, scale[:, :128], scale[:, 128:])
    sh = jnp.where(c == 0, shift[:, :128], shift[:, 128:])
    extra = jnp.concatenate(split3(sc) + split3(sh) + [jnp.zeros((10, 128), F32)], axis=0)
    extra = jnp.concatenate([jnp.zeros((16, 128), F32), extra], axis=1).astype(BF)
    for i in range(8):
        packed[i, 128:144, :] = extra
        packed[i, 0:128, 0:128] = (h[:, i * 128 : (i + 1) * 128].T * gain[...]).astype(BF)
        packed[i, 0:128, 128:256] = conv[i]
    lmine[...] = jnp.where(c == 0, lt[:, :512], lt[:, 512:])
    lother[...] = jnp.where(c == 0, lt[:, 512:], lt[:, :512])


def merge(pos, lam, own, stats, parts, gain, conv, scale, shift):
    return pl.pallas_call(
        merge_kernel,
        out_shape=(
            jax.ShapeDtypeStruct((8, 144, 256), BF),
            jax.ShapeDtypeStruct((2, 512), F32),
            jax.ShapeDtypeStruct((2, 512), F32),
        ),
        in_specs=[smem(), smem()] + [vmem()] * 9,
        out_specs=(vmem(),) * 3,
        compiler_params=pltpu.CompilerParams(vmem_limit_bytes=8 * 1024 * 1024),
        cost_estimate=pl.CostEstimate(flops=500000000, bytes_accessed=4000000, transcendentals=0),
        name="merge",
    )(pos, lam, own, stats, *parts, gain, conv, scale, shift)


def output_kernel(moved, w, out, lhs, held, sem):
    copies = [
        pltpu.make_async_copy(w.at[:, i * 512 : (i + 1) * 512], held.at[i], sem.at[i])
        for i in range(4)
    ]
    for copy in copies:
        copy.start()
    total = jnp.zeros((128, 1), F32)
    square = jnp.zeros((128, 1), F32)
    for i in range(8):
        v = moved[i, 0:128, 128:256].astype(F32)
        total = total + jnp.sum(v, axis=1, keepdims=True)
        square = square + jnp.sum(v * v, axis=1, keepdims=True)
    middle = total * (1.0 / 1024)
    inv = lax.rsqrt(square * (1.0 / 1024) - middle * middle + 1e-05)
    for c in range(2):
        for k in range(4):
            at = k * 256 + c * 128
            p = moved[c * 4 + k, 128:144, 128:256].astype(F32)
            gain = p[0:1] + p[1:2] + p[2:3]
            shift = p[3:4] + p[4:5] + p[5:6]
            lhs[:, at : at + 128] = moved[c * 4 + k, 0:128, 0:128]
            v = moved[c * 4 + k, 0:128, 128:256].astype(F32)
            v = (v - middle) * inv * gain + shift
            lhs[:, 1024 + at : 1152 + at] = (v * jax.nn.sigmoid(v)).astype(BF)
    for i, copy in enumerate(copies):
        copy.wait()
        out[:, i * 512 : (i + 1) * 512] = jnp.dot(
            lhs[...], held[i], preferred_element_type=F32
        ).astype(BF)


def output(moved, w):
    return pl.pallas_call(
        output_kernel,
        out_shape=jax.ShapeDtypeStruct((128, 2048), BF),
        in_specs=[vmem(), pl.BlockSpec(memory_space=pltpu.HBM)],
        out_specs=vmem(),
        scratch_shapes=[
            pltpu.VMEM((128, 2048), BF),
            pltpu.VMEM((4, 2048, 512), BF),
            pltpu.SemaphoreType.DMA((4,)),
        ],
        compiler_params=pltpu.CompilerParams(vmem_limit_bytes=52 * 1024 * 1024),
        cost_estimate=pl.CostEstimate(flops=1100000000, bytes_accessed=9000000, transcendentals=0),
        name="output",
    )(moved, w)


def per_device_steps(
    tokens, norm_gain, query_weight, key_weight, value_weight, glu_value_weight, glu_gate_weight,
    qk_gain, mix_lambda, head_gain, conv_kernel, channel_gain, channel_shift, output_weight,
):
    sp = lax.axis_index("sp").astype(jnp.int32)
    tp = lax.axis_index("tp").astype(jnp.int32)
    core = sp % NC
    pos = jnp.stack([sp // (NY * NC), (sp // NC) % NY, core, tp])
    t1 = along_x(tokens, 1)
    t2 = along_x(tokens, -1)
    t3 = along_x(t1[:64], 1)
    t4 = along_x(t2[64:], -1)
    place = (sp * 512 + jnp.arange(512, dtype=jnp.int32)).astype(F32)
    inverse = 10000.0 ** (-jnp.arange(0, 32, dtype=F32) * 2.0 / 64)
    angles = place[:, None] * inverse[None, :]
    cosine = jnp.cos(angles)
    sine = jnp.sin(angles)
    cos = jnp.concatenate([cosine] * 4, axis=1)
    sin = jnp.concatenate([-sine, sine, -sine, sine], axis=1)
    qkg = jnp.tile(qk_gain.reshape(1, 128), (1, 2))
    t0, *weights = prefetch(
        (tokens, query_weight, key_weight, value_weight, glu_value_weight, glu_gate_weight)
    )
    shared = (
        norm_gain[None, :],
        *weights,
        qkg,
        cos,
        sin,
    )
    filled = project(project_first, 384, pos, (t0, t1, t2), shared, ())
    mine, other = project(project_last, 128, pos, (t3, t4), shared, filled)
    theirs = to_sibling(other)
    both = jnp.where(
        core == 0,
        jnp.concatenate([mine, theirs], axis=1),
        jnp.concatenate([theirs, mine], axis=1),
    )
    q = both[:128]
    kv = both[128:384]
    gated = both[384:]
    halo = lax.ppermute(gated[98:, 896:], "sp", [(i, i + NC) for i in range(NZ * NY * NC - NC)])
    q1 = send_query(q, 1)
    q2 = send_query(q, -1)
    kv1 = send_keys(kv, 1)
    kv2 = send_keys(kv, -1)
    q3 = send_query(q, 2)
    kv3 = send_keys(kv, 2)
    conv = convolve(pos, gated, halo, conv_kernel)
    oacc, tacc = attend_near(pos, (q, q1, q2), (kv, kv1, kv2))
    o3, token = attend_far(pos, q3, (kv, kv1, kv2, kv3), tacc)
    r3 = return_sum(o3, 2)
    own, _, o1, o2, stats = attend_last(pos, (q, q1, q2), (kv, kv1, kv2, kv3), oacc, tacc, token)
    r1 = return_sum(o1, 1)
    r2 = return_sum(o2, -1)
    packed, lmine, lother = merge(
        pos,
        mix_lambda,
        own,
        stats,
        (r1, r2, r3),
        head_gain[None, :],
        conv,
        channel_gain[None, :],
        channel_shift[None, :],
    )
    ltheirs = to_sibling(lother)
    log_totals = jnp.where(
        core == 0, jnp.stack([lmine, ltheirs], axis=1), jnp.stack([ltheirs, lmine], axis=1)
    )
    groups = [
        [(chip * NC + c) * 4 + x for c in range(NC) for x in range(4)] for chip in range(NZ * NY)
    ]
    moved = lax.all_to_all(
        packed, ("sp", "tp"), split_axis=0, concat_axis=0, axis_index_groups=groups, tiled=True
    )
    mixed = output(moved, output_weight)
    return (mixed, log_totals)


def solution(mesh):
    placed = (
        P(("sp", "tp"), None),
        P(),
        P(None, "tp"),
        P(None, "tp"),
        P(None, "tp"),
        P(None, "tp"),
        P(None, "tp"),
        P(),
        P("tp"),
        P(),
        P(None, "tp"),
        P("tp"),
        P("tp"),
        P(),
    )
    return jax.shard_map(
        per_device_steps,
        mesh=mesh,
        in_specs=placed,
        out_specs=(P(("sp", "tp"), None), P(None, "tp", "sp")),
        check_vma=False,
    )
```

profile of v0, /device:TPU:121, one launch (start us, length us, event | category | flops | bytes accessed | tf_op | source)
XLA Modules:
  0.0 196.7 jit_solution(18272089454696141203)
XLA Ops:
  0.6 1.3 collective-permute-start
  1.9 1.5 collective-permute-start.2
  3.4 0.8 tile.10
  4.2 1.0 copy-done.1
  5.2 3.6 %prefetch.1 = (bf16[128,2048]{1,0:T(8,128)(2,1)S(1)}, bf16[2048,256]{1,0:T(8,128)(2,1)S(1)}, bf16[2048,256]{1,0:T(8,128)(2,1)S(1)}, bf16[2048,256]{1,0:T(8,128)(...) custom-call(bf16[128,2048]{1,0:T(8,128)(2,1)S(1)} %copy-done.1, bf16[2048,256]{1,0:T(8,128)(2,1)} %refs_1_.1, ...), custom_call_target="tpu_custom_call" | custom-call | flops 2000000 | bytes 12000000 | tf_op jit(solution)/shard_map/prefetch/pallas_call | solution.py:97
  8.8 0.0 copy-start
  8.8 0.0 copy-start.2
  8.8 1.0 fusion
  9.8 0.5 pad_maximum_fusion
  10.3 4.7 %collective-permute-done.t1 = bf16[128,2048]{1,0:T(8,128)(2,1)S(1)} collective-permute-done((bf16[128,2048]{1,0:T(8,128)(2,1)}, bf16[128,2048]{1,0:T(8,128)(2,1)S(1)}, u32[]{:S(2)}, u32[]{:S(2)}) %collective-permute-start) | collective-permute-done | bytes 524320 | tf_op jit(solution)/shard_map/ppermute | solution.py:78
  14.9 0.1 collective-permute-start.1
  15.0 0.0 collective-permute-done.2.t2
  15.1 2.7 %collective-permute-start.3 = (bf16[64,2048]{1,0:T(8,128)(2,1)S(1)}, bf16[64,2048]{1,0:T(8,128)(2,1)S(1)}, u32[]{:S(2)}, u32[]{:S(2)}) collective-permute-start(bf16[64,2048]{1,0:T(8,128)(2,1)S(1)} %slice.26), channel_id=1, source_target_pairs={{0,3},{1,0},{2,1},{3,2},{4,7},{5,4},{6,5},{7,6},{8,11},{9,8},{10,9... | collective-permute-start | bytes 786440 | tf_op jit(solution)/shard_map/ppermute | solution.py:78
  17.8 0.1 pad_add_fusion.pos
  17.9 0.0 copy-done
  17.9 0.0 copy-done.2
  17.9 4.4 %shard_map.149 = (bf16[512,512]{1,0:T(8,128)(2,1)S(1)}, bf16[512,512]{1,0:T(8,128)(2,1)S(1)}) custom-call(s32[4]{0:T(128)S(1)} %pad_add_fusion.pos, bf16[128,2048]{1,0:T(8,128)(2,1)S(1)} %get-tuple-element.28.t0, bf16[128,2048]{1,0:T(8,128)(2,1)S(1)} %collective-permute-done.t1, bf16[128,2048]{1,0:T(8,128)(2,1)S(1)} %collective-permute-done.2.t2, ...), custom_call_target="tpu_custom_call" | custom-call | flops 2013265920 | bytes 8000000 | tf_op jit(solution)/shard_map/pallas_call | solution.py:185
  22.2 0.3 collective-permute-done.1.t3
  22.6 0.0 collective-permute-done.3.t4
  22.6 2.1 %shard_map.150 = (bf16[512,512]{1,0:T(8,128)(2,1)S(1)}, bf16[512,512]{1,0:T(8,128)(2,1)S(1)}) custom-call(s32[4]{0:T(128)S(1)} %pad_add_fusion.pos, bf16[64,2048]{1,0:T(8,128)(2,1)S(1)} %collective-permute-done.1.t3, bf16[64,2048]{1,0:T(8,128)(2,1)S(1)} %collective-permute-done.3.t4, ...), custom_call_target="tpu_custom_call", output_to_operand_aliasing={{0}: (12, {}), {1}: (13, {})} | custom-call | flops 671088640 | bytes 8000000 | tf_op jit(solution)/shard_map/pallas_call | solution.py:185
  24.7 2.5 %collective-permute-start.4 = (bf16[512,512]{1,0:T(8,128)(2,1)S(1)}, bf16[512,512]{1,0:T(8,128)(2,1)S(1)}, u32[]{:S(2)}, u32[]{:S(2)}) collective-permute-start(bf16[512,512]{1,0:T(8,128)(2,1)S(1)} %get-tuple-element.32), channel_id=1, source_target_pairs={{0,4},{4,0},{8,12},{12,8},{16,20},{20,16},{24,28},{28,24},{32,36},... | collective-permute-start | bytes 1572872 | tf_op jit(solution)/shard_map/ppermute | solution.py:73
  27.2 1.5 collective-permute-done.4
  28.7 0.3 maximum_select_fusion
  29.1 1.3 collective-permute-start.8
  30.4 1.3 collective-permute-start.7
  31.7 6.0 %collective-permute-start.6 = (bf16[128,1024]{1,0:T(8,128)(2,1)S(1)}, bf16[128,1024]{1,0:T(8,128)(2,1)S(1)}, u32[]{:S(2)}, u32[]{:S(2)}) collective-permute-start(bf16[128,1024]{1,0:T(8,128)(2,1)S(1)} %get-tuple-element.49.q0), channel_id=1, source_target_pairs={{8,0},{16,8},{24,16},{32,56},{36,4},{40,32},{44,12},{48,40},{52,20... | collective-permute-start | bytes 786440 | tf_op jit(solution)/shard_map/ppermute | solution.py:53
  37.7 1.3 collective-permute-start.5
  39.0 1.4 collective-permute-start.10
  40.4 0.5 collective-permute-done.6.q2
  40.9 1.3 collective-permute-start.9
  42.2 2.8 %collective-permute-done.5.q1 = bf16[128,1024]{1,0:T(8,128)(2,1)S(1)} collective-permute-done((bf16[128,1024]{1,0:T(8,128)(2,1)S(1)}, bf16[128,1024]{1,0:T(8,128)(2,1)S(1)}, u32[]{:S(2)}, u32[]{:S(2)}) %collective-permute-start.5) | collective-permute-done | bytes 262176 | tf_op jit(solution)/shard_map/ppermute | solution.py:53
  45.1 0.0 collective-permute-done.8.kv2
  45.1 0.0 collective-permute-done.7.kv1
  45.1 7.4 %shard_map.151 = (f32[6,128,1024]{2,1,0:T(8,128)S(1)}, f32[6,8,1024]{2,1,0:T(8,128)S(1)}) custom-call(s32[4]{0:T(128)S(1)} %pad_add_fusion.pos, bf16[128,1024]{1,0:T(8,128)(2,1)S(1)} %get-tuple-element.49.q0, bf16[128,1024]{1,0:T(8,128)(2,1)S(1)} %collective-permute-done.5.q1, bf16[128,1024]{1,0:T(8,128)(2,1)S(1)} %collective-permute-done.6.q2, ...), custom_call_target="tpu_custom_call" | custom-call | flops 6400000000 | bytes 4000000 | tf_op jit(solution)/shard_map/pallas_call | solution.py:465
  52.5 0.0 collective-permute-done.10.q3
  52.5 1.6 collective-permute-done.9.kv3
  54.1 1.2 shard_map.152
  55.3 0.0 copy-start.7
  55.3 21.8 %shard_map.153 = (f32[6,128,1024]{2,1,0:T(8,128)S(1)}, f32[6,8,1024]{2,1,0:T(8,128)S(1)}, bf16[272,1024]{1,0:T(8,128)(2,1)S(1)}, bf16[272,1024]{1,0:T(8,128)(2,1)S(1)}, f32[8,1024]{1,0:T(8,128)S(1)}) custom-call(s32[4]{0:T(128)S(1)} %pad_add_fusion.pos, bf16[128,1024]{1,0:T(8,128)(2,1)S(1)} %get-tuple-element.49.q0, ...), custom_call_target="tpu_custom_call", output_to_operand_aliasing={{0}: (8, {}), {1}: (9, {})} | custom-call | flops 2400000000 | bytes 4000000 | tf_op jit(solution)/shard_map/pallas_call | solution.py:465
  77.2 0.0 copy-start.3
  77.2 0.0 copy-start.4
  77.2 0.0 copy-start.5
  77.2 0.0 copy-start.6
  77.2 1.4 collective-permute-start.11
  78.7 1.3 collective-permute-start.12
  80.0 1.3 collective-permute-start.13
  81.3 1.3 collective-permute-start.14
  82.6 3.1 %collective-permute-done.14.halo = bf16[30,128]{1,0:T(8,128)(2,1)S(1)} collective-permute-done((bf16[30,128]{1,0:T(8,128)(2,1)S(1)}, bf16[30,128]{1,0:T(8,128)(2,1)S(1)}, u32[]{:S(2)}, u32[]{:S(2)}) %collective-permute-start.14) | collective-permute-done | bytes 7712 | tf_op jit(solution)/shard_map/ppermute | solution.py:669
  85.7 0.0 copy-done.7
  85.7 1.6 convolve.1.conv
  87.3 77.1 %collective-permute-done.11.r1 = bf16[272,1024]{1,0:T(8,128)(2,1)S(1)} collective-permute-done((bf16[272,1024]{1,0:T(8,128)(2,1)S(1)}, bf16[272,1024]{1,0:T(8,128)(2,1)S(1)}, u32[]{:S(2)}, u32[]{:S(2)}) %collective-permute-start.11) | collective-permute-done | bytes 557088 | tf_op jit(solution)/shard_map/ppermute | solution.py:61
  164.4 0.0 collective-permute-done.12.r2
  164.4 0.0 collective-permute-done.13.r3
  164.4 0.0 copy-done.3
  164.4 0.0 copy-done.4
  164.4 0.0 copy-done.5
  164.4 0.0 copy-done.6
  164.4 2.2 %merge.1 = (bf16[8,144,256]{2,1,0:T(8,128)(2,1)}, f32[2,512]{1,0:T(2,128)S(1)}, f32[2,512]{1,0:T(2,128)S(1)}) custom-call(s32[4]{0:T(128)S(1)} %pad_add_fusion.pos, f32[2]{0:T(128)S(1)} %copy-done.5, f32[6,128,1024]{2,1,0:T(8,128)S(1)} %get-tuple-element.36.own, f32[8,1024]{1,0:T(8,128)S(1)} %get-tuple-element.37.stats, ...), custom_call_target="tpu_custom_call" | custom-call | flops 500000000 | bytes 4000000 | tf_op jit(solution)/shard_map/merge/pallas_call | solution.py:564
  166.7 15.1 %all-to-all-start = ((bf16[8,144,256]{2,1,0:T(8,128)(2,1)}), bf16[8,144,256]{2,1,0:T(8,128)(2,1)S(1)}, u32[]{:S(2)}, u32[]{:S(2)}) async-start(bf16[8,144,256]{2,1,0:T(8,128)(2,1)} %get-tuple-element.41), calls=%async_computation | async-start | bytes 1179648 | tf_op jit(solution)/shard_map/all_to_all | solution.py:701
  181.7 0.0 collective-permute-start.15
  181.7 1.2 collective-permute-done.15
  182.9 0.6 copy.22
  183.5 8.3 %all-to-all-done.moved = bf16[8,144,256]{2,1,0:T(8,128)(2,1)S(1)} async-done(((bf16[8,144,256]{2,1,0:T(8,128)(2,1)}), bf16[8,144,256]{2,1,0:T(8,128)(2,1)S(1)}, u32[]{:S(2)}, u32[]{:S(2)}) %all-to-all-start) | async-done | bytes 589856 | tf_op jit(solution)/shard_map/all_to_all | solution.py:701
  191.8 4.8 %output.1 = bf16[128,2048]{1,0:T(8,128)(2,1)} custom-call(bf16[8,144,256]{2,1,0:T(8,128)(2,1)S(1)} %all-to-all-done.moved, bf16[2048,2048]{1,0:T(8,128)(2,1)} %w.1), custom_call_target="tpu_custom_call" | custom-call | flops 1100000000 | bytes 9000000 | tf_op jit(solution)/shard_map/output/pallas_call | solution.py:612
  (10 shorter events, 0.1 us)
Async XLA Ops:
  0.6 14.3 %collective-permute-start = (bf16[128,2048]{1,0:T(8,128)(2,1)}, bf16[128,2048]{1,0:T(8,128)(2,1)S(1)}, u32[]{:S(2)}, u32[]{:S(2)}) collective-permute-start(bf16[128,2048]{1,0:T(8,128)(2,1)} %refs_0_.1), channel_id=1, source_target_pairs={{0,1},{1,2},{2,3},{3,0},{4,5},{5,6},{6,7},{7,4},{8,9},{9,10},{10,1... | collective-permute-start | bytes 1572872 | tf_op jit(solution)/shard_map/ppermute | solution.py:78
  1.9 13.1 %collective-permute-start.2 = (bf16[128,2048]{1,0:T(8,128)(2,1)}, bf16[128,2048]{1,0:T(8,128)(2,1)S(1)}, u32[]{:S(2)}, u32[]{:S(2)}) collective-permute-start(bf16[128,2048]{1,0:T(8,128)(2,1)} %refs_0_.1), channel_id=1, source_target_pairs={{0,3},{1,0},{2,1},{3,2},{4,7},{5,4},{6,5},{7,6},{8,11},{9,8},{10,9... | collective-permute-start | bytes 1572872 | tf_op jit(solution)/shard_map/ppermute | solution.py:78
  4.1 1.0 copy-start.1
  8.8 9.1 %copy-start = (bf16[2048,256]{1,0:T(8,128)(2,1)S(1)}, bf16[2048,256]{1,0:T(8,128)(2,1)}, u32[]{:S(2)}) copy-start(bf16[2048,256]{1,0:T(8,128)(2,1)} %get-tuple-element.27.wg) | copy-start | bytes 3145732
  8.8 9.1 %copy-start.2 = (f32[2048]{0:T(1024)S(1)}, f32[2048]{0:T(1024)}, u32[]{:S(2)}) copy-start(f32[2048]{0:T(1024)} %param.15) | copy-start | bytes 24580
  14.9 7.6 %collective-permute-start.1 = (bf16[64,2048]{1,0:T(8,128)(2,1)S(1)}, bf16[64,2048]{1,0:T(8,128)(2,1)S(1)}, u32[]{:S(2)}, u32[]{:S(2)}) collective-permute-start(bf16[64,2048]{1,0:T(8,128)(2,1)S(1)} %slice.25), channel_id=1, source_target_pairs={{0,1},{1,2},{2,3},{3,0},{4,5},{5,6},{6,7},{7,4},{8,9},{9,10},{10,1... | collective-permute-start | bytes 786440 | tf_op jit(solution)/shard_map/ppermute | solution.py:78
  15.1 7.5 %collective-permute-start.3 = (bf16[64,2048]{1,0:T(8,128)(2,1)S(1)}, bf16[64,2048]{1,0:T(8,128)(2,1)S(1)}, u32[]{:S(2)}, u32[]{:S(2)}) collective-permute-start(bf16[64,2048]{1,0:T(8,128)(2,1)S(1)} %slice.26), channel_id=1, source_target_pairs={{0,3},{1,0},{2,1},{3,2},{4,7},{5,4},{6,5},{7,6},{8,11},{9,8},{10,9... | collective-permute-start | bytes 786440 | tf_op jit(solution)/shard_map/ppermute | solution.py:78
  24.7 4.0 %collective-permute-start.4 = (bf16[512,512]{1,0:T(8,128)(2,1)S(1)}, bf16[512,512]{1,0:T(8,128)(2,1)S(1)}, u32[]{:S(2)}, u32[]{:S(2)}) collective-permute-start(bf16[512,512]{1,0:T(8,128)(2,1)S(1)} %get-tuple-element.32), channel_id=1, source_target_pairs={{0,4},{4,0},{8,12},{12,8},{16,20},{20,16},{24,28},{28,24},{32,36},... | collective-permute-start | bytes 1572872 | tf_op jit(solution)/shard_map/ppermute | solution.py:73
  29.1 16.0 %collective-permute-start.8 = (bf16[256,1024]{1,0:T(8,128)(2,1)S(1)}, bf16[256,1024]{1,0:T(8,128)(2,1)S(1)}, u32[]{:S(2)}, u32[]{:S(2)}) collective-permute-start(bf16[256,1024]{1,0:T(8,128)(2,1)S(1)} %slice.28.kv0), channel_id=1, source_target_pairs={{0,96},{4,28},{8,104},{12,4},{16,112},{20,12},{24,120},{28,20},{36... | collective-permute-start | bytes 1572872 | tf_op jit(solution)/shard_map/ppermute | solution.py:69
  30.4 14.7 %collective-permute-start.7 = (bf16[256,1024]{1,0:T(8,128)(2,1)S(1)}, bf16[256,1024]{1,0:T(8,128)(2,1)S(1)}, u32[]{:S(2)}, u32[]{:S(2)}) collective-permute-start(bf16[256,1024]{1,0:T(8,128)(2,1)S(1)} %slice.28.kv0), channel_id=1, source_target_pairs={{0,32},{4,12},{8,40},{12,20},{16,48},{20,28},{24,56},{28,4},{32,64... | collective-permute-start | bytes 1572872 | tf_op jit(solution)/shard_map/ppermute | solution.py:69
  31.7 9.2 %collective-permute-start.6 = (bf16[128,1024]{1,0:T(8,128)(2,1)S(1)}, bf16[128,1024]{1,0:T(8,128)(2,1)S(1)}, u32[]{:S(2)}, u32[]{:S(2)}) collective-permute-start(bf16[128,1024]{1,0:T(8,128)(2,1)S(1)} %get-tuple-element.49.q0), channel_id=1, source_target_pairs={{8,0},{16,8},{24,16},{32,56},{36,4},{40,32},{44,12},{48,40},{52,20... | collective-permute-start | bytes 786440 | tf_op jit(solution)/shard_map/ppermute | solution.py:53
  37.7 7.4 %collective-permute-start.5 = (bf16[128,1024]{1,0:T(8,128)(2,1)S(1)}, bf16[128,1024]{1,0:T(8,128)(2,1)S(1)}, u32[]{:S(2)}, u32[]{:S(2)}) collective-permute-start(bf16[128,1024]{1,0:T(8,128)(2,1)S(1)} %get-tuple-element.49.q0), channel_id=1, source_target_pairs={{24,0},{32,40},{40,48},{48,56},{56,32},{64,72},{72,80},{80,88},{88... | collective-permute-start | bytes 786440 | tf_op jit(solution)/shard_map/ppermute | solution.py:53
  39.0 13.5 %collective-permute-start.10 = (bf16[128,1024]{1,0:T(8,128)(2,1)S(1)}, bf16[128,1024]{1,0:T(8,128)(2,1)S(1)}, u32[]{:S(2)}, u32[]{:S(2)}) collective-permute-start(bf16[128,1024]{1,0:T(8,128)(2,1)S(1)} %get-tuple-element.49.q0), channel_id=1, source_target_pairs={{16,0},{24,8},{32,48},{40,56},{48,32},{56,40},{64,80},{68,4},{72,8... | collective-permute-start | bytes 786440 | tf_op jit(solution)/shard_map/ppermute | solution.py:53
  40.9 13.2 %collective-permute-start.9 = (bf16[256,1024]{1,0:T(8,128)(2,1)S(1)}, bf16[256,1024]{1,0:T(8,128)(2,1)S(1)}, u32[]{:S(2)}, u32[]{:S(2)}) collective-permute-start(bf16[256,1024]{1,0:T(8,128)(2,1)S(1)} %slice.28.kv0), channel_id=1, source_target_pairs={{0,64},{4,20},{8,72},{12,28},{16,80},{20,4},{24,88},{28,12},{32,96... | collective-permute-start | bytes 1572872 | tf_op jit(solution)/shard_map/ppermute | solution.py:69
  55.3 30.4 %copy-start.7 = (f32[31,256]{1,0:T(8,128)S(1)}, f32[31,256]{1,0:T(8,128)}, u32[]{:S(2)}) copy-start(f32[31,256]{1,0:T(8,128)} %taps.1) | copy-start | bytes 95236
  77.2 87.2 %copy-start.3 = (f32[256]{0:T(256)S(1)}, f32[256]{0:T(256)}, u32[]{:S(2)}) copy-start(f32[256]{0:T(256)} %param.25) | copy-start | bytes 3076
  77.2 87.2 %copy-start.4 = (f32[256]{0:T(256)S(1)}, f32[256]{0:T(256)}, u32[]{:S(2)}) copy-start(f32[256]{0:T(256)} %param.26) | copy-start | bytes 3076
  77.2 87.2 %copy-start.5 = (f32[2]{0:T(128)S(1)}, f32[2]{0:T(128)}, u32[]{:S(2)}) copy-start(f32[2]{0:T(128)} %lam.1) | copy-start | bytes 28
  77.2 87.2 %copy-start.6 = (f32[128]{0:T(128)S(1)}, f32[128]{0:T(128)}, u32[]{:S(2)}) copy-start(f32[128]{0:T(128)} %param.23) | copy-start | bytes 1540
  77.2 87.2 %collective-permute-start.11 = (bf16[272,1024]{1,0:T(8,128)(2,1)S(1)}, bf16[272,1024]{1,0:T(8,128)(2,1)S(1)}, u32[]{:S(2)}, u32[]{:S(2)}) collective-permute-start(bf16[272,1024]{1,0:T(8,128)(2,1)S(1)} %get-tuple-element.38), channel_id=1, source_target_pairs={{0,24},{4,100},{12,108},{20,116},{28,124},{32,56},{40,32},{48,40},... | collective-permute-start | bytes 1671176 | tf_op jit(solution)/shard_map/ppermute | solution.py:61
  78.7 85.7 %collective-permute-start.12 = (bf16[272,1024]{1,0:T(8,128)(2,1)S(1)}, bf16[272,1024]{1,0:T(8,128)(2,1)S(1)}, u32[]{:S(2)}, u32[]{:S(2)}) collective-permute-start(bf16[272,1024]{1,0:T(8,128)(2,1)S(1)} %get-tuple-element.39), channel_id=1, source_target_pairs={{0,8},{4,36},{8,16},{12,44},{16,24},{20,52},{28,60},{32,40},{36,68... | collective-permute-start | bytes 1671176 | tf_op jit(solution)/shard_map/ppermute | solution.py:61
  80.0 84.4 %collective-permute-start.13 = (bf16[272,1024]{1,0:T(8,128)(2,1)S(1)}, bf16[272,1024]{1,0:T(8,128)(2,1)S(1)}, u32[]{:S(2)}, u32[]{:S(2)}) collective-permute-start(bf16[272,1024]{1,0:T(8,128)(2,1)S(1)} %get-tuple-element.40), channel_id=1, source_target_pairs={{0,16},{4,68},{8,24},{12,76},{20,84},{28,92},{32,48},{36,100},{40,... | collective-permute-start | bytes 1671176 | tf_op jit(solution)/shard_map/ppermute | solution.py:61
  81.3 4.4 %collective-permute-start.14 = (bf16[30,128]{1,0:T(8,128)(2,1)S(1)}, bf16[30,128]{1,0:T(8,128)(2,1)S(1)}, u32[]{:S(2)}, u32[]{:S(2)}) collective-permute-start(bf16[30,128]{1,0:T(8,128)(2,1)S(1)} %slice.30), channel_id=1, source_target_pairs={{0,8},{4,12},{8,16},{12,20},{16,24},{20,28},{24,32},{28,36},{32,40... | collective-permute-start | bytes 23048 | tf_op jit(solution)/shard_map/ppermute | solution.py:669
  166.7 25.1 %all-to-all-start = ((bf16[8,144,256]{2,1,0:T(8,128)(2,1)}), bf16[8,144,256]{2,1,0:T(8,128)(2,1)S(1)}, u32[]{:S(2)}, u32[]{:S(2)}) async-start(bf16[8,144,256]{2,1,0:T(8,128)(2,1)} %get-tuple-element.41), calls=%async_computation | async-start | bytes 1179648 | tf_op jit(solution)/shard_map/all_to_all | solution.py:701
  181.7 1.2 collective-permute-start.15
where the time goes:
time: 201 us; the launch traced here: 197 us
  waiting for transfers between devices  101 us (50%)
  Pallas kernels  49.1 us (24%)
  starting transfers between devices  40.9 us (20%)
  local copies, waits for them, and re-layouts  2.57 us (1%)
    ppermute x3, waiting for transfers between devices, return_sum(): return lax.ppermute(value, 'sp', moves(target))  77.1 us
    pallas_call x3, Pallas kernels, attention_call(): pl.pallas_call(body, out_shape=outs, in_specs=[smem()] + [vmem()] * (len(...  30.4 us
    all_to_all x1, starting transfers between devices, per_device_steps(): lax.all_to_all(packed, ('sp', 'tp'), split_axis=0, concat_axis=0, axis_in...  15.1 us
    ppermute x3, starting transfers between devices, send_query(): return lax.ppermute(value, 'sp', moves(target))  8.7 us
    all_to_all x1, waiting for transfers between devices, per_device_steps(): lax.all_to_all(packed, ('sp', 'tp'), split_axis=0, concat_axis=0, axis_in...  8.26 us
    pallas_call x2, Pallas kernels, project(): pl.pallas_call(body, out_shape=(jax.ShapeDtypeStruct((512, 512), BF), jax...  6.49 us
    ppermute x4, starting transfers between devices, along_x(): lax.ppermute(value, 'tp', [(i, (i + step) % count) for i in range(count)])  5.54 us
    ppermute x4, waiting for transfers between devices, along_x(): lax.ppermute(value, 'tp', [(i, (i + step) % count) for i in range(count)])  4.99 us
  transfers between devices with their start and end apart: 17, of which 10 were waited for; matrix products, arithmetic and copies ran while one was open for 2% of the time, Pallas kernels for 9%

commit v1 on v0

v1 whole, which is shorter than its diff:
```python
import math

import jax
import jax.numpy as jnp
from jax import lax
from jax.experimental import pallas as pl
from jax.experimental.pallas import tpu as pltpu
from jax.sharding import PartitionSpec as P

NZ, NY, NC = 4, 4, 2
BIG = 2.0**100
LOG2E = math.log2(math.e)
BF = jnp.bfloat16
F32 = jnp.float32


def vmem():
    return pl.BlockSpec(memory_space=pltpu.VMEM)


def smem():
    return pl.BlockSpec(memory_space=pltpu.SMEM)


def moves(target):
    out = []
    for z in range(NZ):
        for y in range(NY):
            for c in range(NC):
                t = target(z, y, c)
                if t is not None:
                    out.append(((z * NY + y) * NC + c, (t[0] * NY + t[1]) * NC + t[2]))
    return out


def stepped(z, y, along_y, step):
    return (z, (y + step) % NY) if along_y else ((z + step) % NZ, y)


def send_query(value, step):
    return lax.ppermute(
        value, "sp", moves(lambda z, y, c: (*stepped(z, y, c == 0, step), c))
    )


def send_keys(value, step):
    return lax.ppermute(
        value, "sp", moves(lambda z, y, c: (*stepped(z, y, c == 1, step), c))
    )


def to_mirror(value):
    return lax.ppermute(value, "sp", moves(lambda z, y, c: (NZ - 1 - z, y, 1 - c)))


def along_x(value, step):
    count = lax.axis_size("tp")
    return lax.ppermute(value, "tp", [(i, (i + step) % count) for i in range(count)])


def hbm():
    return pl.BlockSpec(memory_space=pl.ANY)


def prefetch_kernel(*refs):
    n = (len(refs) - 3) // 2
    copies = [
        pltpu.make_async_copy(refs[i], refs[n + 2 + i], refs[2 * n + 2].at[i]) for i in range(n)
    ]
    for copy in copies:
        copy.start()
    for copy in copies:
        copy.wait()


def prefetch(arrays, *tables):
    return pl.pallas_call(
        prefetch_kernel,
        out_shape=tuple(jax.ShapeDtypeStruct(a.shape, a.dtype) for a in arrays),
        in_specs=[hbm()] * len(arrays) + [vmem()] * 2,
        out_specs=(vmem(),) * len(arrays),
        scratch_shapes=[pltpu.SemaphoreType.DMA((len(arrays),))],
        compiler_params=pltpu.CompilerParams(vmem_limit_bytes=48 * 1024 * 1024),
        cost_estimate=pl.CostEstimate(flops=2000000, bytes_accessed=12000000, transcendentals=0),
        name="prefetch",
    )(*arrays, *tables)


def project_body(pos, pieces, gain, ws, qkg, cos, sin, mine, other, gated, normed):
    x = pos[3]
    c = pos[2]
    ats = []
    row = 0
    for ref, step in pieces:
        t = ref[...].astype(F32)
        n = t.shape[0]
        ms = jnp.mean(t * t, axis=-1, keepdims=True)
        normed[row : row + n, :] = (t * lax.rsqrt(ms + 1e-06) * gain[...]).astype(BF)
        if row % 128 == 0:
            ats.append(pl.multiple_of(lax.rem(x + step, 4) * 128, 128))
        row += n
    lane = lax.broadcasted_iota(jnp.int32, (1, 256), 1)
    first = lax.rem(lane, 64) < 32
    gi = lax.broadcasted_iota(jnp.int32, (256, 256), 0) // 64
    gj = lax.broadcasted_iota(jnp.int32, (256, 256), 1) // 64
    groups = jnp.where(gi == gj, 1.0 / 64, 0.0).astype(BF)

    def table(ref):
        v = jnp.concatenate([ref[pl.ds(at, 128), :] for at in ats], axis=0)
        return jnp.concatenate([v, v], axis=1)

    cc = table(cos)
    ss = table(sin)

    def times(w):
        return jnp.dot(normed[...], w[...], preferred_element_type=F32).astype(BF).astype(F32)

    def turned(w):
        v = times(w)
        sq = v * v
        hi = sq.astype(BF)
        lo = (sq - hi.astype(F32)).astype(BF)
        ms = jnp.dot(hi, groups, preferred_element_type=F32) + jnp.dot(
            lo, groups, preferred_element_type=F32
        )
        v = v * lax.rsqrt(ms + 1e-06) * qkg[...]
        swapped = jnp.where(first, pltpu.roll(v, 256 - 32, 1), pltpu.roll(v, 32, 1))
        return v * cc + swapped * ss

    def put(row, v, flip):
        a = v[:, :128]
        b = v[:, 128:]
        kept = jnp.where(c == 0, a, b)
        given = jnp.where(c == 0, b, a)
        for i, at in enumerate(ats):
            rows = slice(i * 128, (i + 1) * 128)
            part = kept[rows, :]
            mine[row : row + 128, pl.ds(at, 128)] = (part.T if flip else part).astype(BF)
            part = given[rows, :]
            other[row : row + 128, rows] = (part.T if flip else part).astype(BF)

    wq, wk, wv, wa, wg = ws
    put(0, turned(wq) * (LOG2E / 8.0), True)
    put(128, turned(wk), False)
    put(256, times(wv), True)
    g = times(wa) * jax.nn.sigmoid(times(wg))
    for i, at in enumerate(ats):
        gated[pl.ds(at, 128), :] = g[i * 128 : (i + 1) * 128, :].astype(BF)


def project_first(
    pos, t0, a1, b1, b2, a2, gain, wq, wk, wv, wa, wg, qkg, cos, sin, mine, gated, other, normed
):
    project_body(
        pos, ((t0, 0), (a1, 3), (b1, 3), (b2, 1), (a2, 1)), gain, (wq, wk, wv, wa, wg), qkg, cos,
        sin, mine, other, gated, normed,
    )


def project_last(
    pos, f1, f2, gain, wq, wk, wv, wa, wg, qkg, cos, sin, mine_in, gated_in, mine, gated, other,
    normed,
):
    project_body(
        pos, ((f1, 2), (f2, 2)), gain, (wq, wk, wv, wa, wg), qkg, cos, sin,
        mine, other, gated, normed,
    )


def project(body, rows, pos, pieces, shared, filled):
    count = 1 + len(pieces) + len(shared) + len(filled)
    start = count - len(filled)
    return pl.pallas_call(
        body,
        out_shape=(
            jax.ShapeDtypeStruct((384, 512), BF),
            jax.ShapeDtypeStruct((512, 256), BF),
            jax.ShapeDtypeStruct((384, rows), BF),
        ),
        in_specs=[smem()] + [vmem()] * (count - 1),
        out_specs=(vmem(),) * 3,
        scratch_shapes=[pltpu.VMEM((rows, 2048), BF)],
        input_output_aliases={start + i: i for i in range(len(filled))},
        compiler_params=pltpu.CompilerParams(vmem_limit_bytes=14 * 1024 * 1024),
        cost_estimate=pl.CostEstimate(
            flops=5242880 * rows, bytes_accessed=8000000, transcendentals=0
        ),
    )(pos, *pieces, *shared, *filled)


def assemble_kernel(pos, mine, near, far, q, kv):
    x = pos[3]
    q[:, 0:512] = mine[0:128, :]
    kv[:, 0:512] = mine[128:384, :]
    for i, step in enumerate((0, 3, 1, 2)):
        at = pl.multiple_of(512 + lax.rem(x + step, 4) * 128, 128)
        ref = near if i < 3 else far
        cols = slice(i * 128, (i + 1) * 128) if i < 3 else slice(0, 128)
        q[:, pl.ds(at, 128)] = ref[0:128, cols]
        kv[:, pl.ds(at, 128)] = ref[128:384, cols]


def assemble(pos, mine, near, far):
    return pl.pallas_call(
        assemble_kernel,
        out_shape=(
            jax.ShapeDtypeStruct((128, 1024), BF),
            jax.ShapeDtypeStruct((256, 1024), BF),
        ),
        in_specs=[smem()] + [vmem()] * 3,
        out_specs=(vmem(),) * 2,
        compiler_params=pltpu.CompilerParams(vmem_limit_bytes=4 * 1024 * 1024),
        cost_estimate=pl.CostEstimate(flops=1000000, bytes_accessed=1500000, transcendentals=0),
        name="assemble",
    )(pos, mine, near, far)


def conv_kernel_body(gated, halo, taps, scale, shift, out, ext):
    ext[0:32, :] = jnp.zeros((32, 256), F32)
    ext[544:560, :] = jnp.zeros((16, 256), F32)
    ext[2:32, :] = halo[...].astype(F32)
    ext[32:544, :] = gated[...].astype(F32)
    for lanes in (slice(0, 128), slice(128, 256)):
        for i in range(4):
            acc = jnp.zeros((128, 128), F32)
            for r in range(8):
                moved = ext[i * 128 + r : i * 128 + r + 160, lanes]
                for a in range(5):
                    j = a * 8 + r - 2
                    if 0 <= j < 31:
                        acc = acc + taps[j : j + 1, lanes] * moved[8 * a : 8 * a + 128]
            out[i, 0:128, lanes] = acc.astype(BF)
    extra = split3(scale[...]) + split3(shift[...]) + [jnp.zeros((10, 256), F32)]
    extra = jnp.concatenate(extra, axis=0).astype(BF)
    for i in range(4):
        out[i, 128:144, :] = extra


def convolve(gated, halo, taps, scale, shift):
    return pl.pallas_call(
        conv_kernel_body,
        out_shape=jax.ShapeDtypeStruct((4, 144, 256), BF),
        in_specs=[vmem()] * 5,
        out_specs=vmem(),
        scratch_shapes=[pltpu.VMEM((560, 256), F32)],
        compiler_params=pltpu.CompilerParams(vmem_limit_bytes=4 * 1024 * 1024),
        cost_estimate=pl.CostEstimate(flops=1000000000, bytes_accessed=800000, transcendentals=0),
        name="convolve",
    )(gated, halo, taps, scale, shift)


def split3(v):
    hi = v.astype(BF).astype(F32)
    mid = (v - hi).astype(BF).astype(F32)
    return [hi, mid, v - hi - mid]


def spans(pos):
    z, y, c = pos[0], pos[1], pos[2]

    def halves(z, y):
        return (z * 4 + y) * 2 + c, ((3 - z) * 4 + y) * 2 + 1 - c

    own = halves(z, y)
    over_y = [own] + [halves(z, lax.rem(y + d, 4)) for d in (3, 1, 2)]
    over_z = [own] + [halves(lax.rem(z + d, 4), y) for d in (3, 1, 2)]

    def pick(p, q):
        return [tuple(jnp.where(c == 0, u, v) for u, v in zip(m, n)) for m, n in zip(p, q)]

    return pick(over_y, over_z), pick(over_z, over_y)


def load_query(ref, qz, s):
    rows = lax.broadcasted_iota(jnp.int32, (128, 512), 0)
    for i in range(2):
        q = ref[:, i * 512 : (i + 1) * 512]
        qz[4 * s + 2 * i] = jnp.where(rows < 64, q, jnp.zeros_like(q))
        qz[4 * s + 2 * i + 1] = jnp.where(rows >= 64, q, jnp.zeros_like(q))


def load_keys(ref, kscr, vscr, b):
    for i in range(8):
        at = (i % 4) * 128
        kscr[2 * b + i // 4, at : at + 128, :] = ref[0:128, i * 128 : (i + 1) * 128]
    for j in range(2):
        vscr[2 * b + j] = ref[128:256, j * 512 : (j + 1) * 512]


def list_pairs(todo, pairs, queries, keys):
    n = jnp.int32(0)
    todo[0] = 0
    for s, b in pairs:
        for i in range(2):
            for j in range(2):
                ok = keys[b][j] < queries[s][i]
                code = s * 16 + i * 8 + b * 2 + j

                @pl.when(ok)
                def _(n=n, code=code):
                    todo[n] = code
                    todo[n + 1] = code

                n = n + ok.astype(jnp.int32)
    return n


def weigh(tacc, mref, r, cols, scores, masked):
    n, w = scores.shape
    s3 = scores.reshape(n // 8, 8, w)
    if mref is not None:
        s3 = s3 - mref[r, :, cols][None]
    p = jnp.exp2(s3).reshape(n, w)
    if masked:
        k = lax.broadcasted_iota(jnp.int32, (256, 256), 0)
        q = lax.broadcasted_iota(jnp.int32, (256, 256), 1)
        last = jnp.where(k <= q, p[n - 256 :], 0.0)
        p = last if n == 256 else jnp.concatenate([p[: n - 256], last], axis=0)
    tacc[r, :, cols] += jnp.sum(p.reshape(n // 8, 8, w), axis=0)
    return p.astype(BF)


def run_pairs(todo, n, qz, kscr, vscr, sbuf, pbuf, oacc, tacc, mref):
    def score(e, m):
        return jnp.dot(kscr[e & 7], qz[(e >> 3) * 2 + m], preferred_element_type=F32)

    @pl.when(n > 0)
    def _():
        sbuf[0] = score(todo[0], 0)

        @pl.loop(0, n)
        def _(t):
            e = todo[t]
            later = todo[t + 1]
            for m in range(2):
                sbuf[1 - m] = score(e, 1) if m == 0 else score(later, 0)
                r = (e >> 3) * 2 + m
                pbuf[m] = weigh(tacc, mref, r, slice(0, 512), sbuf[m], False)
                oacc[r] += jnp.dot(vscr[e & 7], pbuf[m], preferred_element_type=F32)


def run_diagonal(qz, kscr, vscr, sbuf, pbuf, oacc, tacc, mref):
    for h in range(2):
        for m in range(2):
            for qt in range(2):
                n = (qt + 1) * 256
                cols = slice(qt * 256, n)
                r = h * 2 + m
                sbuf[m, :n, cols] = jnp.dot(
                    kscr[h, :n, :], qz[r, :, cols], preferred_element_type=F32
                )
                pbuf[m, :n, cols] = weigh(tacc, mref, r, cols, sbuf[m, :n, cols], True)
                oacc[r, :, cols] += jnp.dot(
                    vscr[h, :, :n], pbuf[m, :n, cols], preferred_element_type=F32
                )


def take_tops(todo, n, sources, qz, kscr, tacc, mref):
    for s in sources:
        tacc[4 * s : 4 * s + 4] = jnp.full((4, 8, 512), -1e30, F32)

    def one(b, r, qt, masked):
        cols = pl.ds(pl.multiple_of(qt * 256, 256), 256)
        sc = jnp.dot(kscr[b], qz[r, :, cols], preferred_element_type=F32)
        if masked:
            k = lax.broadcasted_iota(jnp.int32, (512, 256), 0)
            q = lax.broadcasted_iota(jnp.int32, (512, 256), 1) + qt * 256
            sc = jnp.where(k <= q, sc, -1e30)
        tacc[r, :, cols] = jnp.maximum(tacc[r, :, cols], jnp.max(sc.reshape(64, 8, 256), axis=0))

    if 0 in sources:

        @pl.loop(0, 8)
        def _(i):
            one(i >> 2, i >> 1, i & 1, True)

    @pl.loop(0, n * 4)
    def _(i):
        e = todo[i >> 2]
        one(e & 7, (e >> 3) * 2 + ((i >> 1) & 1), i & 1, False)

    for s in sources:
        for r in range(4 * s, 4 * s + 4):
            mref[r] = jnp.broadcast_to(jnp.max(tacc[r], axis=0, keepdims=True), (8, 512))


def finish(sources, fast, pos, qz, kvs, kscr, vscr, sbuf, pbuf, oacc, tacc, mref, todo, flag):
    queries, keys = spans(pos)
    mref[...] = jnp.zeros_like(mref)
    flag[0] = 1

    @pl.loop(0, 2)
    def _(attempt):
        @pl.when(flag[0] == 1)
        def _():
            flag[1] = list_pairs(todo, fast, queries, keys)

            @pl.when(attempt == 1)
            def _():
                for b in range(4):
                    load_keys(kvs[b], kscr, vscr, b)
                every = [(s, b) for s in sources for b in range(4)]
                flag[1] = list_pairs(todo, every, queries, keys)
                take_tops(todo, flag[1], sources, qz, kscr, tacc, mref)
                for s in sources:
                    oacc[4 * s : 4 * s + 4] = jnp.zeros((4, 128, 512), F32)
                    tacc[4 * s : 4 * s + 4] = jnp.zeros((4, 8, 512), F32)
                if 0 in sources:
                    run_diagonal(qz, kscr, vscr, sbuf, pbuf, oacc, tacc, mref)

            run_pairs(todo, flag[1], qz, kscr, vscr, sbuf, pbuf, oacc, tacc, mref)
            worst = jnp.zeros((1, 512), F32)
            for s in sources:
                for i in range(2):
                    has = s == 0
                    for b in range(4):
                        for j in range(2):
                            has = jnp.logical_or(has, keys[b][j] < queries[s][i])
                    least = jnp.where(has, 1.0 / BIG, -1.0)
                    for m in range(2):
                        t = jnp.sum(tacc[4 * s + 2 * i + m], axis=0, keepdims=True)
                        good = jnp.logical_and(t < BIG, t > least)
                        worst = jnp.where(good, worst, 1.0)
            bad = (jnp.max(worst) > 0.5).astype(jnp.int32)
            flag[0] = jnp.where(attempt == 0, bad, 0)


def gathered(ref, s, m, axis):
    pieces = [ref[4 * s + 2 * i + m] for i in range(2)]
    if axis is not None:
        pieces = [jnp.sum(p, axis=0, keepdims=True) for p in pieces]
    return jnp.concatenate(pieces, axis=1)


def write_sum(ref, s, oacc, tacc, mref):
    extra = []
    for m in range(2):
        ref[m * 128 : (m + 1) * 128, :] = gathered(oacc, s, m, None).astype(BF)
        extra = extra + split3(gathered(tacc, s, m, 0))
    for m in range(2):
        extra = extra + split3(gathered(mref, s, m, None)[0:1])
    ref[256:272, :] = jnp.concatenate(extra + [jnp.zeros((4, 1024), F32)], axis=0).astype(BF)


def own_kernel(pos, q0, kv0, oacc, tacc, qz, kscr, vscr, sbuf, pbuf, todo):
    load_query(q0, qz, 0)
    load_keys(kv0, kscr, vscr, 0)
    oacc[...] = jnp.zeros_like(oacc)
    tacc[...] = jnp.zeros_like(tacc)
    run_diagonal(qz, kscr, vscr, sbuf, pbuf, oacc, tacc, None)


def near_kernel(
    pos, q0, q1, q2, kv0, kv1, kv2, oin, tin, oacc, tacc, qz, kscr, vscr, sbuf, pbuf, todo
):
    queries, keys = spans(pos)
    for s, ref in enumerate((q0, q1, q2)):
        load_query(ref, qz, s)
    for b, ref in enumerate((kv0, kv1, kv2)):
        load_keys(ref, kscr, vscr, b)
    n = list_pairs(todo, [(s, b) for b in range(3) for s in range(3)], queries, keys)
    run_pairs(todo, n, qz, kscr, vscr, sbuf, pbuf, oacc, tacc, None)


def mid_kernel(
    pos, q1, q2, kv0, kv1, kv2, kv3, oin, tin, oacc, tacc, out1, out2,
    qz, kscr, vscr, sbuf, pbuf, todo, mref, flag,
):
    for s, ref in enumerate((q1, q2)):
        load_query(ref, qz, s + 1)
    kvs = (kv0, kv1, kv2, kv3)
    load_keys(kv3, kscr, vscr, 3)
    fast = [(1, 3), (2, 3)]
    finish((1, 2), fast, pos, qz, kvs, kscr, vscr, sbuf, pbuf, oacc, tacc, mref, todo, flag)
    write_sum(out1, 1, oacc, tacc, mref)
    write_sum(out2, 2, oacc, tacc, mref)


def far_kernel(
    pos, q3, kv0, kv1, kv2, kv3, oin, tin, oacc, tacc, out3,
    qz, kscr, vscr, sbuf, pbuf, todo, mref, flag,
):
    load_query(q3, qz, 3)
    kvs = (kv0, kv1, kv2, kv3)
    for b in range(4):
        load_keys(kvs[b], kscr, vscr, b)
    fast = [(3, b) for b in range(4)]
    finish((3,), fast, pos, qz, kvs, kscr, vscr, sbuf, pbuf, oacc, tacc, mref, todo, flag)
    write_sum(out3, 3, oacc, tacc, mref)


def last_kernel(
    pos, q0, kv0, kv1, kv2, kv3, oin, tin, own, stats,
    qz, kscr, vscr, sbuf, pbuf, todo, mref, flag, tacc,
):
    own[...] = oin[0:4]
    tacc[...] = tin[0:4]
    load_query(q0, qz, 0)
    kvs = (kv0, kv1, kv2, kv3)
    load_keys(kv3, kscr, vscr, 3)
    finish((0,), [(0, 3)], pos, qz, kvs, kscr, vscr, sbuf, pbuf, own, tacc, mref, todo, flag)
    t = [gathered(tacc, 0, m, 0) for m in range(2)]
    top = [gathered(mref, 0, m, None)[0:1] for m in range(2)]
    stats[...] = jnp.concatenate(t + top + [jnp.zeros((4, 1024), F32)], axis=0)


def attention_call(body, ins, outs, pairs, carried=True, checked=True, sums=None, extra=()):
    sums = sums or (jax.ShapeDtypeStruct((16, 128, 512), F32), jax.ShapeDtypeStruct((16, 8, 512), F32))
    scratches = [
        pltpu.VMEM((16, 128, 512), BF),
        pltpu.VMEM((8, 512, 128), BF),
        pltpu.VMEM((8, 128, 512), BF),
        pltpu.VMEM((2, 512, 512), F32),
        pltpu.VMEM((2, 512, 512), BF),
        pltpu.SMEM((72,), jnp.int32),
    ]
    if checked:
        scratches += [pltpu.VMEM((16, 8, 512), F32), pltpu.SMEM((2,), jnp.int32), *extra]
    return pl.pallas_call(
        body,
        out_shape=(*sums, *outs),
        in_specs=[smem()] + [vmem()] * (len(ins) - 1),
        out_specs=(vmem(),) * (2 + len(outs)),
        scratch_shapes=scratches,
        input_output_aliases={len(ins) - 2: 0, len(ins) - 1: 1} if carried else {},
        compiler_params=pltpu.CompilerParams(vmem_limit_bytes=12 * 1024 * 1024),
        cost_estimate=pl.CostEstimate(
            flops=800000000 * pairs, bytes_accessed=4000000, transcendentals=2000000 * pairs
        ),
    )(*ins)


SENT = jax.ShapeDtypeStruct((272, 1024), BF)


def merge_kernel(pos, lam, own, stats, r1, r2, r3, gain, packed, lmine, lother):
    c = pos[2]
    mix = jnp.where(c == 0, lam[0], lam[1])

    def joined(ref, row):
        part = ref[256:272, :].astype(F32)
        return part[row : row + 1] + part[row + 1 : row + 2] + part[row + 2 : row + 3]

    heads = []
    logs = []
    for m in range(2):
        ts = [stats[m : m + 1, :]] + [joined(r, 3 * m) for r in (r1, r2, r3)]
        ms = [stats[2 + m : 3 + m, :]] + [joined(r, 6 + 3 * m) for r in (r1, r2, r3)]
        ms = [jnp.where(t > 0, v, -1e30) for t, v in zip(ts, ms)]
        top = jnp.maximum(jnp.maximum(ms[0], ms[1]), jnp.maximum(ms[2], ms[3]))
        ws = [jnp.exp2(v - top) for v in ms]
        total = ws[0] * ts[0] + ws[1] * ts[1] + ws[2] * ts[2] + ws[3] * ts[3]
        inv = 1.0 / total
        acc = jnp.concatenate([own[m], own[2 + m]], axis=1) * (ws[0] * inv)
        for w, r in zip(ws[1:], (r1, r2, r3)):
            acc = acc + r[m * 128 : (m + 1) * 128, :].astype(F32) * (w * inv)
        heads.append(acc)
        logs.append(top * math.log(2.0) + jnp.log(total))
    h = heads[0] - mix * heads[1]
    h = h * lax.rsqrt(jnp.mean(h * h, axis=0, keepdims=True) + 1e-06)
    lt = jnp.concatenate(logs, axis=0)
    for i in range(8):
        u = (i // 4) * 512 + (i % 4) * 128
        v = (1 - i // 4) * 512 + (i % 4) * 128
        part = jnp.where(c == 0, h[:, u : u + 128], h[:, v : v + 128])
        packed[i] = (part.T * gain[...]).astype(BF)
    lmine[...] = lt[:, :512]
    lother[...] = lt[:, 512:]


def merge(pos, lam, own, stats, parts, *rest):
    return pl.pallas_call(
        merge_kernel,
        out_shape=(
            jax.ShapeDtypeStruct((8, 128, 128), BF),
            jax.ShapeDtypeStruct((2, 512), F32),
            jax.ShapeDtypeStruct((2, 512), F32),
        ),
        in_specs=[smem(), smem()] + [vmem()] * 6,
        out_specs=(vmem(),) * 3,
        compiler_params=pltpu.CompilerParams(vmem_limit_bytes=8 * 1024 * 1024),
        cost_estimate=pl.CostEstimate(flops=500000000, bytes_accessed=4000000, transcendentals=0),
        name="merge",
    )(pos, lam, own, stats, *parts, *rest)


def fetches(w, first, held, sem):
    copies = [
        pltpu.make_async_copy(
            w.at[first : first + 1024, i * 512 : (i + 1) * 512], held.at[i], sem.at[i]
        )
        for i in range(4)
    ]
    for copy in copies:
        copy.start()
    return copies


def half_kernel(moved, token, w, out, lhs, held, sem):
    copies = fetches(w, 1024, held, sem)
    total = jnp.zeros((128, 1), F32)
    square = jnp.zeros((128, 1), F32)
    for k in range(4):
        v = moved[k, 0:128, :].astype(F32)
        total = total + jnp.sum(v, axis=1, keepdims=True)
        square = square + jnp.sum(v * v, axis=1, keepdims=True)
    middle = total * (1.0 / 1024)
    inv = lax.rsqrt(square * (1.0 / 1024) - middle * middle + 1e-05)
    for k in range(4):
        p = moved[k, 128:144, :].astype(F32)
        gain = p[0:1] + p[1:2] + p[2:3]
        shift = p[3:4] + p[4:5] + p[5:6]
        v = moved[k, 0:128, :].astype(F32)
        v = (v - middle) * inv * gain + shift
        lhs[:, k * 256 : (k + 1) * 256] = (v * jax.nn.sigmoid(v)).astype(BF)
    for i, copy in enumerate(copies):
        copy.wait()
        out[:, i * 512 : (i + 1) * 512] = jnp.dot(lhs[...], held[i], preferred_element_type=F32)


def output_kernel(moved, part, w, out, lhs, held, sem):
    copies = fetches(w, 0, held, sem)
    for c in range(2):
        for k in range(4):
            at = k * 256 + c * 128
            lhs[:, at : at + 128] = moved[c * 4 + k]
    for i, copy in enumerate(copies):
        copy.wait()
        cols = slice(i * 512, (i + 1) * 512)
        out[:, cols] = (
            part[:, cols] + jnp.dot(lhs[...], held[i], preferred_element_type=F32)
        ).astype(BF)


def product(body, dtype, moved, other, w):
    return pl.pallas_call(
        body,
        out_shape=jax.ShapeDtypeStruct((128, 2048), dtype),
        in_specs=[vmem(), vmem(), hbm()],
        out_specs=vmem(),
        scratch_shapes=[
            pltpu.VMEM((128, 1024), BF),
            pltpu.VMEM((4, 1024, 512), BF),
            pltpu.SemaphoreType.DMA((4,)),
        ],
        compiler_params=pltpu.CompilerParams(vmem_limit_bytes=52 * 1024 * 1024),
        cost_estimate=pl.CostEstimate(flops=600000000, bytes_accessed=5000000, transcendentals=0),
    )(moved, other, w)


def per_device_steps(
    tokens, norm_gain, query_weight, key_weight, value_weight, glu_value_weight, glu_gate_weight,
    qk_gain, mix_lambda, head_gain, conv_kernel, channel_gain, channel_shift, output_weight,
):
    sp = lax.axis_index("sp").astype(jnp.int32)
    tp = lax.axis_index("tp").astype(jnp.int32)
    core = sp % NC
    pos = jnp.stack([sp // (NY * NC), (sp // NC) % NY, core, tp])
    upper, lower = tokens[:64], tokens[64:]
    a1 = along_x(upper, 1)
    a2 = along_x(lower, -1)
    b1 = along_x(lower, 1)
    b2 = along_x(upper, -1)
    f1 = along_x(a1, 1)
    f2 = along_x(a2, -1)
    place = (sp * 512 + jnp.arange(512, dtype=jnp.int32)).astype(F32)
    inverse = 10000.0 ** (-jnp.arange(0, 32, dtype=F32) * 2.0 / 64)
    angles = place[:, None] * inverse[None, :]
    cosine = jnp.cos(angles)
    sine = jnp.sin(angles)
    cos = jnp.concatenate([cosine] * 4, axis=1)
    sin = jnp.concatenate([-sine, sine, -sine, sine], axis=1)
    qkg = jnp.tile(qk_gain.reshape(1, 128), (1, 2))
    t0, *weights = prefetch(
        (tokens, query_weight, key_weight, value_weight, glu_value_weight, glu_gate_weight),
        cos,
        sin,
    )
    shared = (
        norm_gain[None, :],
        *weights,
        qkg,
        cos,
        sin,
    )
    mine, gated, given = project(project_first, 384, pos, (t0, a1, b1, b2, a2), shared, ())
    near_in = to_mirror(given)
    mine, gated, given = project(project_last, 128, pos, (f1, f2), shared, (mine, gated))
    far_in = to_mirror(given)
    halo = lax.ppermute(
        gated[482:], "sp", [(i, i + 1) for i in range(NZ * NY * NC - 1)]
    )
    q, kv = assemble(pos, mine, near_in, far_in)
    kv1 = send_keys(kv, 1)
    kv2 = send_keys(kv, -1)
    q1 = send_query(q, 1)
    q2 = send_query(q, -1)
    q3 = send_query(q, 2)
    kv3 = send_keys(kv, 2)
    sums = attention_call(own_kernel, (pos, q, kv), (), 1, carried=False, checked=False)
    sums = attention_call(near_kernel, (pos, q, q1, q2, kv, kv1, kv2, *sums), (), 8, checked=False)
    *sums, o1, o2 = attention_call(
        mid_kernel, (pos, q1, q2, kv, kv1, kv2, kv3, *sums), (SENT,) * 2, 2
    )
    r1 = send_query(o1, -1)
    r2 = send_query(o2, 1)
    *sums, o3 = attention_call(far_kernel, (pos, q3, kv, kv1, kv2, kv3, *sums), (SENT,), 4)
    r3 = send_query(o3, 2)
    own, stats = attention_call(
        last_kernel,
        (pos, q, kv, kv1, kv2, kv3, *sums),
        (),
        1,
        carried=False,
        sums=(
            jax.ShapeDtypeStruct((4, 128, 512), F32),
            jax.ShapeDtypeStruct((8, 1024), F32),
        ),
        extra=(pltpu.VMEM((4, 8, 512), F32),),
    )
    conv = convolve(gated, halo, conv_kernel, channel_gain[None, :], channel_shift[None, :])
    conv, stats = lax.optimization_barrier((conv, stats))
    conv = lax.all_to_all(conv, "tp", split_axis=0, concat_axis=0, tiled=True)
    packed, lmine, lother = merge(
        pos,
        mix_lambda,
        own,
        stats,
        (r1, r2, r3),
        head_gain[None, :],
    )
    groups = []
    for z in range(NZ):
        for y in range(NY):
            ends = ((z * NY + y) * NC, ((NZ - 1 - z) * NY + y) * NC + 1)
            groups.append([end * 4 + x for end in ends for x in range(4)])
    moved = lax.all_to_all(
        packed, ("sp", "tp"), split_axis=0, concat_axis=0, axis_index_groups=groups, tiled=True
    )
    ltheirs = to_mirror(lother)
    log_totals = jnp.where(
        core == 0, jnp.stack([lmine, ltheirs], axis=1), jnp.stack([ltheirs, lmine], axis=1)
    )
    part = product(half_kernel, F32, conv, lmine, output_weight)
    mixed = product(output_kernel, BF, moved, part, output_weight)
    return (mixed, log_totals)


def solution(mesh):
    placed = (
        P(("sp", "tp"), None),
        P(),
        P(None, "tp"),
        P(None, "tp"),
        P(None, "tp"),
        P(None, "tp"),
        P(None, "tp"),
        P(),
        P("tp"),
        P(),
        P(None, "tp"),
        P("tp"),
        P("tp"),
        P(),
    )
    return jax.shard_map(
        per_device_steps,
        mesh=mesh,
        in_specs=placed,
        out_specs=(P(("sp", "tp"), None), P(None, "tp", "sp")),
        check_vma=False,
    )
```

time: 201 us -> 192 us (0.955)
  the two profiles are of different devices: /device:TPU:121 before, /device:TPU:1 now
where the time goes in v1:
time: 192 us
  Pallas kernels  89.1 us (46%)
  starting transfers between devices  76 us (40%)
  waiting for transfers between devices  19.1 us (10%)
  local copies, waits for them, and re-layouts  4.72 us (2%)
    pallas_call x5, Pallas kernels, attention_call(): pl.pallas_call(body, out_shape=(*sums, *outs), in_specs=[smem()] + [vmem(...  67.4 us
    ppermute x1, starting transfers between devices, per_device_steps(): lax.ppermute(gated[482:], 'sp', [(i, i + 1) for i in range(NZ * NY * NC -...  22.1 us
    all_to_all x1, starting transfers between devices, per_device_steps(): lax.all_to_all(packed, ('sp', 'tp'), split_axis=0, concat_axis=0, axis_in...  16.5 us
    ppermute x6, starting transfers between devices, send_query(): lax.ppermute(value, 'sp', moves(lambda z, y, c: (*stepped(z, y, c == 0, s...  14.3 us
    ppermute x6, starting transfers between devices, along_x(): lax.ppermute(value, 'tp', [(i, (i + step) % count) for i in range(count)])  8.74 us
    ppermute x3, waiting for transfers between devices, to_mirror(): lax.ppermute(value, 'sp', moves(lambda z, y, c: (NZ - 1 - z, y, 1 - c)))  7.38 us
    pallas_call x2, Pallas kernels, project(): pl.pallas_call(body, out_shape=(jax.ShapeDtypeStruct((384, 512), BF), jax...  6.5 us
    ppermute x3, starting transfers between devices, to_mirror(): lax.ppermute(value, 'sp', moves(lambda z, y, c: (NZ - 1 - z, y, 1 - c)))  6.38 us
  transfers between devices with their start and end apart: 21, of which 8 were waited for; matrix products, arithmetic and copies ran while one was open for 2% of the time, Pallas kernels for 34%

profile of v1, /device:TPU:1, one launch (start us, length us, event | category | flops | bytes accessed | tf_op | source)
XLA Modules:
  0.0 191.6 jit_solution(6042150645134103482)
XLA Ops:
  0.6 1.1 fusion.1
  1.7 3.4 %collective-permute-start.2 = (bf16[64,2048]{1,0:T(8,128)(2,1)S(1)}, bf16[64,2048]{1,0:T(8,128)(2,1)S(1)}, u32[]{:S(2)}, u32[]{:S(2)}) collective-permute-start(bf16[64,2048]{1,0:T(8,128)(2,1)S(1)} %get-tuple-element.70), channel_id=1, source_target_pairs={{0,3},{1,0},{2,1},{3,2},{4,7},{5,4},{6,5},{7,6},{8,11},{9,8},{10,9... | collective-permute-start | bytes 786440 | tf_op jit(solution)/shard_map/ppermute | solution.py:58
  5.1 0.0 collective-permute-start.4
  5.1 0.2 collective-permute-start
  5.3 2.5 %collective-permute-start.5 = (bf16[64,2048]{1,0:T(8,128)(2,1)S(1)}, bf16[64,2048]{1,0:T(8,128)(2,1)S(1)}, u32[]{:S(2)}, u32[]{:S(2)}) collective-permute-start(bf16[64,2048]{1,0:T(8,128)(2,1)S(1)} %get-tuple-element.71), channel_id=1, source_target_pairs={{0,3},{1,0},{2,1},{3,2},{4,7},{5,4},{6,5},{7,6},{8,11},{9,8},{10,9... | collective-permute-start | bytes 786440 | tf_op jit(solution)/shard_map/ppermute | solution.py:58
  7.8 1.0 fusion
  8.8 0.8 tile.10
  9.6 0.5 pad_maximum_fusion
  10.1 0.0 copy-start
  10.1 1.0 copy-done
  11.1 3.6 %prefetch.1 = (bf16[128,2048]{1,0:T(8,128)(2,1)S(1)}, bf16[2048,256]{1,0:T(8,128)(2,1)S(1)}, bf16[2048,256]{1,0:T(8,128)(2,1)S(1)}, bf16[2048,256]{1,0:T(8,128)(...) custom-call(bf16[128,2048]{1,0:T(8,128)(2,1)S(1)} %copy-done, bf16[2048,256]{1,0:T(8,128)(2,1)} %refs_1_.1, ...), custom_call_target="tpu_custom_call" | custom-call | flops 2000000 | bytes 12000000 | tf_op jit(solution)/shard_map/prefetch/pallas_call | solution.py:77
  14.7 0.1 pad_add_fusion.pos
  14.8 4.0 %collective-permute-done.a1 = bf16[64,2048]{1,0:T(8,128)(2,1)S(1)} collective-permute-done((bf16[64,2048]{1,0:T(8,128)(2,1)S(1)}, bf16[64,2048]{1,0:T(8,128)(2,1)S(1)}, u32[]{:S(2)}, u32[]{:S(2)}) %collective-permute-start) | collective-permute-done | bytes 262176 | tf_op jit(solution)/shard_map/ppermute | solution.py:58
  18.8 0.0 collective-permute-start.1
  18.8 0.0 collective-permute-done.2.a2
  18.8 2.7 %collective-permute-start.3 = (bf16[64,2048]{1,0:T(8,128)(2,1)S(1)}, bf16[64,2048]{1,0:T(8,128)(2,1)S(1)}, u32[]{:S(2)}, u32[]{:S(2)}) collective-permute-start(bf16[64,2048]{1,0:T(8,128)(2,1)S(1)} %collective-permute-done.2.a2), channel_id=1, source_target_pairs={{0,3},{1,0},{2,1},{3,2},{4,7},{5,4},{6,5},{7,6},{8,11},{9,8},{10,9... | collective-permute-start | bytes 786440 | tf_op jit(solution)/shard_map/ppermute | solution.py:58
  21.5 0.0 collective-permute-done.4.b1
  21.5 0.0 collective-permute-done.5.b2
  21.5 1.2 copy-done.1
  22.7 4.4 %shard_map.149 = (bf16[384,512]{1,0:T(8,128)(2,1)S(1)}, bf16[512,256]{1,0:T(8,128)(2,1)S(1)}, bf16[384,384]{1,0:T(8,128)(2,1)S(1)}) custom-call(s32[4]{0:T(128)S(1)} %pad_add_fusion.pos, bf16[128,2048]{1,0:T(8,128)(2,1)S(1)} %get-tuple-element.39.t0, bf16[64,2048]{1,0:T(8,128)(2,1)S(1)} %collective-permute-done.a1, ...), custom_call_target="tpu_custom_call" | custom-call | flops 2013265920 | bytes 8000000 | tf_op jit(solution)/shard_map/pallas_call | solution.py:173
  27.1 6.1 %collective-permute-start.6 = (bf16[384,384]{1,0:T(8,128)(2,1)S(1)}, bf16[384,384]{1,0:T(8,128)(2,1)S(1)}, u32[]{:S(2)}, u32[]{:S(2)}) collective-permute-start(bf16[384,384]{1,0:T(8,128)(2,1)S(1)} %get-tuple-element.43), channel_id=1, source_target_pairs={{0,100},{4,96},{8,108},{12,104},{16,116},{20,112},{24,124},{28,120... | collective-permute-start | bytes 884744 | tf_op jit(solution)/shard_map/ppermute | solution.py:53
  33.2 0.0 collective-permute-done.1.f1
  33.2 0.0 collective-permute-done.3.f2
  33.2 2.1 %shard_map.150 = (bf16[384,512]{1,0:T(8,128)(2,1)S(1)}, bf16[512,256]{1,0:T(8,128)(2,1)S(1)}, bf16[384,128]{1,0:T(8,128)(2,1)S(1)}) custom-call(s32[4]{0:T(128)S(1)} %pad_add_fusion.pos, bf16[64,2048]{1,0:T(8,128)(2,1)S(1)} %collective-permute-done.1.f1, ...), custom_call_target="tpu_custom_call", output_to_operand_aliasing={{0}: (12, {}), {1}: (13, {})} | custom-call | flops 671088640 | bytes 8000000 | tf_op jit(solution)/shard_map/pallas_call | solution.py:173
  35.3 0.1 collective-permute-start.7
  35.5 5.0 %collective-permute-done.6.near = bf16[384,384]{1,0:T(8,128)(2,1)S(1)} collective-permute-done((bf16[384,384]{1,0:T(8,128)(2,1)S(1)}, bf16[384,384]{1,0:T(8,128)(2,1)S(1)}, u32[]{:S(2)}, u32[]{:S(2)}) %collective-permute-start.6) | collective-permute-done | bytes 294944 | tf_op jit(solution)/shard_map/ppermute | solution.py:53
  40.4 1.1 collective-permute-done.7.far
  41.5 0.7 assemble.1
  42.2 1.4 collective-permute-start.8
  43.5 1.5 collective-permute-start.9
  45.1 0.4 collective-permute-start.12
  45.5 2.3 %collective-permute-start.13 = (bf16[128,1024]{1,0:T(8,128)(2,1)S(1)}, bf16[128,1024]{1,0:T(8,128)(2,1)S(1)}, u32[]{:S(2)}, u32[]{:S(2)}) collective-permute-start(bf16[128,1024]{1,0:T(8,128)(2,1)S(1)} %get-tuple-element.45.q0), channel_id=1, source_target_pairs={{0,24},{4,100},{8,0},{12,108},{16,8},{20,116},{24,16},{28,124},{32... | collective-permute-start | bytes 786440 | tf_op jit(solution)/shard_map/ppermute | solution.py:41
  47.7 1.6 collective-permute-start.10
  49.3 2.4 %shard_map.151 = (f32[16,128,512]{2,1,0:T(8,128)S(1)}, f32[16,8,512]{2,1,0:T(8,128)S(1)}) custom-call(s32[4]{0:T(128)S(1)} %pad_add_fusion.pos, bf16[128,1024]{1,0:T(8,128)(2,1)S(1)} %get-tuple-element.45.q0, bf16[256,1024]{1,0:T(8,128)(2,1)S(1)} %get-tuple-element.46.kv0), custom_call_target="tpu_custom_call" | custom-call | flops 800000000 | bytes 4000000 | tf_op jit(solution)/shard_map/pallas_call | solution.py:519
  51.7 2.9 %collective-permute-done.12.q1 = bf16[128,1024]{1,0:T(8,128)(2,1)S(1)} collective-permute-done((bf16[128,1024]{1,0:T(8,128)(2,1)S(1)}, bf16[128,1024]{1,0:T(8,128)(2,1)S(1)}, u32[]{:S(2)}, u32[]{:S(2)}) %collective-permute-start.12) | collective-permute-done | bytes 262176 | tf_op jit(solution)/shard_map/ppermute | solution.py:41
  54.6 0.0 collective-permute-start.11
  54.6 0.0 collective-permute-done.13.q2
  54.6 0.0 collective-permute-done.8.kv1
  54.6 0.0 collective-permute-done.9.kv2
  54.6 8.8 %shard_map.152 = (f32[16,128,512]{2,1,0:T(8,128)S(1)}, f32[16,8,512]{2,1,0:T(8,128)S(1)}) custom-call(s32[4]{0:T(128)S(1)} %pad_add_fusion.pos, bf16[128,1024]{1,0:T(8,128)(2,1)S(1)} %get-tuple-element.45.q0, bf16[128,1024]{1,0:T(8,128)(2,1)S(1)} %collective-permute-done.12.q1, ...), custom_call_target="tpu_custom_call", output_to_operand_aliasing={{0}: (7, {}), {1}: (8, {})} | custom-call | flops 6400000000 | bytes 4000000 | tf_op jit(solution)/shard_map/pallas_call | solution.py:519
  63.4 0.0 collective-permute-done.10.kv3
  63.4 24.4 %shard_map.153 = (f32[16,128,512]{2,1,0:T(8,128)S(1)}, f32[16,8,512]{2,1,0:T(8,128)S(1)}, bf16[272,1024]{1,0:T(8,128)(2,1)}, bf16[272,1024]{1,0:T(8,128)(2,1)}) custom-call(s32[4]{0:T(128)S(1)} %pad_add_fusion.pos, bf16[128,1024]{1,0:T(8,128)(2,1)S(1)} %collective-permute-done.12.q1, ...), custom_call_target="tpu_custom_call", output_to_operand_aliasing={{0}: (7, {}), {1}: (8, {})} | custom-call | flops 1600000000 | bytes 4000000 | tf_op jit(solution)/shard_map/pallas_call | solution.py:519
  87.8 0.0 collective-permute-done.11.q3
  87.8 0.0 copy-start.7
  87.8 19.7 %shard_map.154 = (f32[16,128,512]{2,1,0:T(8,128)S(1)}, f32[16,8,512]{2,1,0:T(8,128)S(1)}, bf16[272,1024]{1,0:T(8,128)(2,1)}) custom-call(s32[4]{0:T(128)S(1)} %pad_add_fusion.pos, bf16[128,1024]{1,0:T(8,128)(2,1)S(1)} %collective-permute-done.11.q3, bf16[256,1024]{1,0:T(8,128)(2,1)S(1)} %get-tuple-element.46.kv0, ...), custom_call_target="tpu_custom_call", output_to_operand_aliasing={{0}: (6, {}), {1}: (7, {})} | custom-call | flops 3200000000 | bytes 4000000 | tf_op jit(solution)/shard_map/pallas_call | solution.py:519
  107.5 3.0 %collective-permute-start.17 = (bf16[272,1024]{1,0:T(8,128)(2,1)}, bf16[272,1024]{1,0:T(8,128)(2,1)S(1)}, u32[]{:S(2)}, u32[]{:S(2)}) collective-permute-start(bf16[272,1024]{1,0:T(8,128)(2,1)} %get-tuple-element.61), channel_id=1, source_target_pairs={{0,16},{4,68},{8,24},{12,76},{16,0},{20,84},{24,8},{28,92},{32,48}... | collective-permute-start | bytes 1671176 | tf_op jit(solution)/shard_map/ppermute | solution.py:41
  110.5 8.1 %collective-permute-start.15 = (bf16[272,1024]{1,0:T(8,128)(2,1)}, bf16[272,1024]{1,0:T(8,128)(2,1)S(1)}, u32[]{:S(2)}, u32[]{:S(2)}) collective-permute-start(bf16[272,1024]{1,0:T(8,128)(2,1)} %get-tuple-element.59), channel_id=1, source_target_pairs={{0,24},{4,100},{8,0},{12,108},{16,8},{20,116},{24,16},{28,124},{32... | collective-permute-start | bytes 1671176 | tf_op jit(solution)/shard_map/ppermute | solution.py:41
  118.6 0.6 collective-permute-start.16
  119.2 22.1 %collective-permute-start.14 = (bf16[30,256]{1,0:T(8,128)(2,1)S(1)}, bf16[30,256]{1,0:T(8,128)(2,1)S(1)}, u32[]{:S(2)}, u32[]{:S(2)}) collective-permute-start(bf16[30,256]{1,0:T(8,128)(2,1)S(1)} %slice.11), channel_id=1, source_target_pairs={{0,4},{4,8},{8,12},{12,16},{16,20},{20,24},{24,28},{28,32},{32,36}... | collective-permute-start | bytes 46088 | tf_op jit(solution)/shard_map/ppermute | solution.py:690
  141.4 0.6 collective-permute-done.14.halo
  142.0 2.8 %convolve.1 = bf16[4,144,256]{2,1,0:T(8,128)(2,1)} custom-call(bf16[512,256]{1,0:T(8,128)(2,1)S(1)} %get-tuple-element.56.gated, bf16[30,256]{1,0:T(8,128)(2,1)S(1)} %collective-permute-done.14.halo, f32[31,256]{1,0:T(8,128)S(1)} %copy-done.5, f32[1,256]{1,0:T(1,128)S(1)} %bitcast.17, f32[1,256]{1,0:T(1,128)S(1)} %bitcast.18), custom_call_target="tpu_custom_call" | custom-call | flops 1000000000 | bytes 800000 | tf_op jit(solution)/shard_map/convolve/pallas_call | solution.py:240
  144.8 12.1 %shard_map.155 = (f32[4,128,512]{2,1,0:T(8,128)S(1)}, f32[8,1024]{1,0:T(8,128)S(1)}) custom-call(s32[4]{0:T(128)S(1)} %pad_add_fusion.pos, bf16[128,1024]{1,0:T(8,128)(2,1)S(1)} %get-tuple-element.45.q0, bf16[256,1024]{1,0:T(8,128)(2,1)S(1)} %get-tuple-element.46.kv0, bf16[256,1024]{1,0:T(8,128)(2,1)S(1)} %collective-permute-done.8.kv1, ...), custom_call_target="tpu_custom_call" | custom-call | flops 800000000 | bytes 4000000 | tf_op jit(solution)/shard_map/pallas_call | solution.py:519
  156.9 3.5 %all-to-all-start.1 = ((bf16[4,144,256]{2,1,0:T(8,128)(2,1)}), bf16[4,144,256]{2,1,0:T(8,128)(2,1)S(1)}, u32[]{:S(2)}, u32[]{:S(2)}) async-start(bf16[4,144,256]{2,1,0:T(8,128)(2,1)} %convolve.1), calls=%async_computation.1 | async-start | bytes 589824 | tf_op jit(solution)/shard_map/all_to_all | solution.py:723
  160.4 0.0 collective-permute-done.17.r3
  160.4 0.0 collective-permute-done.15.r1
  160.5 2.2 %merge.1 = (bf16[8,128,128]{2,1,0:T(8,128)(2,1)}, f32[2,512]{1,0:T(2,128)S(1)}, f32[2,512]{1,0:T(2,128)S(1)}) custom-call(s32[4]{0:T(128)S(1)} %pad_add_fusion.pos, f32[2]{0:T(128)S(1)} %copy-done.3, f32[4,128,512]{2,1,0:T(8,128)S(1)} %get-tuple-element.55.own, f32[8,1024]{1,0:T(8,128)S(1)} %get-tuple-element.58.stats, ...), custom_call_target="tpu_custom_call" | custom-call | flops 500000000 | bytes 4000000 | tf_op jit(solution)/shard_map/merge/pallas_call | solution.py:572
  162.6 3.5 %all-to-all-done.1.moved = bf16[4,144,256]{2,1,0:T(8,128)(2,1)S(1)} async-done(((bf16[4,144,256]{2,1,0:T(8,128)(2,1)}), bf16[4,144,256]{2,1,0:T(8,128)(2,1)S(1)}, u32[]{:S(2)}, u32[]{:S(2)}) %all-to-all-start.1) | async-done | bytes 294944 | tf_op jit(solution)/shard_map/all_to_all | solution.py:723
  166.1 16.5 %all-to-all-start = ((bf16[8,128,128]{2,1,0:T(8,128)(2,1)}), bf16[8,128,128]{2,1,0:T(8,128)(2,1)S(1)}, u32[]{:S(2)}, u32[]{:S(2)}) async-start(bf16[8,128,128]{2,1,0:T(8,128)(2,1)} %get-tuple-element.62), calls=%async_computation | async-start | bytes 524288 | tf_op jit(solution)/shard_map/all_to_all | solution.py:737
  182.6 0.2 collective-permute-start.18
  182.7 2.7 %shard_map.156.part = f32[128,2048]{1,0:T(8,128)S(1)} custom-call(bf16[4,144,256]{2,1,0:T(8,128)(2,1)S(1)} %all-to-all-done.1.moved, f32[2,512]{1,0:T(2,128)S(1)} %get-tuple-element.64.token, bf16[2048,2048]{1,0:T(8,128)(2,1)} %w.3), custom_call_target="tpu_custom_call" | custom-call | flops 600000000 | bytes 5000000 | tf_op jit(solution)/shard_map/pallas_call | solution.py:636
  185.5 1.3 collective-permute-done.18
  186.8 0.6 copy.26
  187.4 0.7 all-to-all-done.moved
  188.1 3.3 %shard_map.157 = bf16[128,2048]{1,0:T(8,128)(2,1)} custom-call(bf16[8,128,128]{2,1,0:T(8,128)(2,1)S(1)} %all-to-all-done.moved, f32[128,2048]{1,0:T(8,128)S(1)} %shard_map.156.part, bf16[2048,2048]{1,0:T(8,128)(2,1)} %w.3), custom_call_target="tpu_custom_call" | custom-call | flops 600000000 | bytes 5000000 | tf_op jit(solution)/shard_map/pallas_call | solution.py:636
  (18 shorter events, 0.1 us)
Async XLA Ops:
  1.7 17.1 %collective-permute-start.2 = (bf16[64,2048]{1,0:T(8,128)(2,1)S(1)}, bf16[64,2048]{1,0:T(8,128)(2,1)S(1)}, u32[]{:S(2)}, u32[]{:S(2)}) collective-permute-start(bf16[64,2048]{1,0:T(8,128)(2,1)S(1)} %get-tuple-element.70), channel_id=1, source_target_pairs={{0,3},{1,0},{2,1},{3,2},{4,7},{5,4},{6,5},{7,6},{8,11},{9,8},{10,9... | collective-permute-start | bytes 786440 | tf_op jit(solution)/shard_map/ppermute | solution.py:58
  5.1 16.4 %collective-permute-start.4 = (bf16[64,2048]{1,0:T(8,128)(2,1)S(1)}, bf16[64,2048]{1,0:T(8,128)(2,1)S(1)}, u32[]{:S(2)}, u32[]{:S(2)}) collective-permute-start(bf16[64,2048]{1,0:T(8,128)(2,1)S(1)} %get-tuple-element.70), channel_id=1, source_target_pairs={{0,1},{1,2},{2,3},{3,0},{4,5},{5,6},{6,7},{7,4},{8,9},{9,10},{10,1... | collective-permute-start | bytes 786440 | tf_op jit(solution)/shard_map/ppermute | solution.py:58
  5.1 13.7 %collective-permute-start = (bf16[64,2048]{1,0:T(8,128)(2,1)S(1)}, bf16[64,2048]{1,0:T(8,128)(2,1)S(1)}, u32[]{:S(2)}, u32[]{:S(2)}) collective-permute-start(bf16[64,2048]{1,0:T(8,128)(2,1)S(1)} %get-tuple-element.71), channel_id=1, source_target_pairs={{0,1},{1,2},{2,3},{3,0},{4,5},{5,6},{6,7},{7,4},{8,9},{9,10},{10,1... | collective-permute-start | bytes 786440 | tf_op jit(solution)/shard_map/ppermute | solution.py:58
  5.3 16.2 %collective-permute-start.5 = (bf16[64,2048]{1,0:T(8,128)(2,1)S(1)}, bf16[64,2048]{1,0:T(8,128)(2,1)S(1)}, u32[]{:S(2)}, u32[]{:S(2)}) collective-permute-start(bf16[64,2048]{1,0:T(8,128)(2,1)S(1)} %get-tuple-element.71), channel_id=1, source_target_pairs={{0,3},{1,0},{2,1},{3,2},{4,7},{5,4},{6,5},{7,6},{8,11},{9,8},{10,9... | collective-permute-start | bytes 786440 | tf_op jit(solution)/shard_map/ppermute | solution.py:58
  7.8 13.7 %copy-start.2 = (f32[2048]{0:T(1024)S(1)}, f32[2048]{0:T(1024)}, u32[]{:S(2)}) copy-start(f32[2048]{0:T(1024)} %param.15) | copy-start | bytes 24580
  10.1 1.0 copy-start
  18.8 14.4 %collective-permute-start.1 = (bf16[64,2048]{1,0:T(8,128)(2,1)S(1)}, bf16[64,2048]{1,0:T(8,128)(2,1)S(1)}, u32[]{:S(2)}, u32[]{:S(2)}) collective-permute-start(bf16[64,2048]{1,0:T(8,128)(2,1)S(1)} %collective-permute-done.a1), channel_id=1, source_target_pairs={{0,1},{1,2},{2,3},{3,0},{4,5},{5,6},{6,7},{7,4},{8,9},{9,10},{10,1... | collective-permute-start | bytes 786440 | tf_op jit(solution)/shard_map/ppermute | solution.py:58
  18.8 14.4 %collective-permute-start.3 = (bf16[64,2048]{1,0:T(8,128)(2,1)S(1)}, bf16[64,2048]{1,0:T(8,128)(2,1)S(1)}, u32[]{:S(2)}, u32[]{:S(2)}) collective-permute-start(bf16[64,2048]{1,0:T(8,128)(2,1)S(1)} %collective-permute-done.2.a2), channel_id=1, source_target_pairs={{0,3},{1,0},{2,1},{3,2},{4,7},{5,4},{6,5},{7,6},{8,11},{9,8},{10,9... | collective-permute-start | bytes 786440 | tf_op jit(solution)/shard_map/ppermute | solution.py:58
  21.5 1.2 copy-start.1
  27.1 13.3 %collective-permute-start.6 = (bf16[384,384]{1,0:T(8,128)(2,1)S(1)}, bf16[384,384]{1,0:T(8,128)(2,1)S(1)}, u32[]{:S(2)}, u32[]{:S(2)}) collective-permute-start(bf16[384,384]{1,0:T(8,128)(2,1)S(1)} %get-tuple-element.43), channel_id=1, source_target_pairs={{0,100},{4,96},{8,108},{12,104},{16,116},{20,112},{24,124},{28,120... | collective-permute-start | bytes 884744 | tf_op jit(solution)/shard_map/ppermute | solution.py:53
  35.3 6.1 %collective-permute-start.7 = (bf16[384,128]{1,0:T(8,128)(2,1)S(1)}, bf16[384,128]{1,0:T(8,128)(2,1)S(1)}, u32[]{:S(2)}, u32[]{:S(2)}) collective-permute-start(bf16[384,128]{1,0:T(8,128)(2,1)S(1)} %get-tuple-element.44), channel_id=1, source_target_pairs={{0,100},{4,96},{8,108},{12,104},{16,116},{20,112},{24,124},{28,120... | collective-permute-start | bytes 294920 | tf_op jit(solution)/shard_map/ppermute | solution.py:53
  42.2 12.4 %collective-permute-start.8 = (bf16[256,1024]{1,0:T(8,128)(2,1)S(1)}, bf16[256,1024]{1,0:T(8,128)(2,1)S(1)}, u32[]{:S(2)}, u32[]{:S(2)}) collective-permute-start(bf16[256,1024]{1,0:T(8,128)(2,1)S(1)} %get-tuple-element.46.kv0), channel_id=1, source_target_pairs={{0,32},{4,12},{8,40},{12,20},{16,48},{20,28},{24,56},{28,4},{32,64... | collective-permute-start | bytes 1572872 | tf_op jit(solution)/shard_map/ppermute | solution.py:47
  43.5 11.1 %collective-permute-start.9 = (bf16[256,1024]{1,0:T(8,128)(2,1)S(1)}, bf16[256,1024]{1,0:T(8,128)(2,1)S(1)}, u32[]{:S(2)}, u32[]{:S(2)}) collective-permute-start(bf16[256,1024]{1,0:T(8,128)(2,1)S(1)} %get-tuple-element.46.kv0), channel_id=1, source_target_pairs={{0,96},{4,28},{8,104},{12,4},{16,112},{20,12},{24,120},{28,20},{32... | collective-permute-start | bytes 1572872 | tf_op jit(solution)/shard_map/ppermute | solution.py:47
  45.1 9.5 %collective-permute-start.12 = (bf16[128,1024]{1,0:T(8,128)(2,1)S(1)}, bf16[128,1024]{1,0:T(8,128)(2,1)S(1)}, u32[]{:S(2)}, u32[]{:S(2)}) collective-permute-start(bf16[128,1024]{1,0:T(8,128)(2,1)S(1)} %get-tuple-element.45.q0), channel_id=1, source_target_pairs={{0,8},{4,36},{8,16},{12,44},{16,24},{20,52},{24,0},{28,60},{32,40}... | collective-permute-start | bytes 786440 | tf_op jit(solution)/shard_map/ppermute | solution.py:41
  45.5 9.1 %collective-permute-start.13 = (bf16[128,1024]{1,0:T(8,128)(2,1)S(1)}, bf16[128,1024]{1,0:T(8,128)(2,1)S(1)}, u32[]{:S(2)}, u32[]{:S(2)}) collective-permute-start(bf16[128,1024]{1,0:T(8,128)(2,1)S(1)} %get-tuple-element.45.q0), channel_id=1, source_target_pairs={{0,24},{4,100},{8,0},{12,108},{16,8},{20,116},{24,16},{28,124},{32... | collective-permute-start | bytes 786440 | tf_op jit(solution)/shard_map/ppermute | solution.py:41
  47.7 15.7 %collective-permute-start.10 = (bf16[256,1024]{1,0:T(8,128)(2,1)S(1)}, bf16[256,1024]{1,0:T(8,128)(2,1)S(1)}, u32[]{:S(2)}, u32[]{:S(2)}) collective-permute-start(bf16[256,1024]{1,0:T(8,128)(2,1)S(1)} %get-tuple-element.46.kv0), channel_id=1, source_target_pairs={{0,64},{4,20},{8,72},{12,28},{16,80},{20,4},{24,88},{28,12},{32,96... | collective-permute-start | bytes 1572872 | tf_op jit(solution)/shard_map/ppermute | solution.py:47
  54.6 33.2 %collective-permute-start.11 = (bf16[128,1024]{1,0:T(8,128)(2,1)S(1)}, bf16[128,1024]{1,0:T(8,128)(2,1)S(1)}, u32[]{:S(2)}, u32[]{:S(2)}) collective-permute-start(bf16[128,1024]{1,0:T(8,128)(2,1)S(1)} %get-tuple-element.45.q0), channel_id=1, source_target_pairs={{0,16},{4,68},{8,24},{12,76},{16,0},{20,84},{24,8},{28,92},{32,48}... | collective-permute-start | bytes 786440 | tf_op jit(solution)/shard_map/ppermute | solution.py:41
  87.8 54.2 %copy-start.5 = (f32[31,256]{1,0:T(8,128)S(1)}, f32[31,256]{1,0:T(8,128)}, u32[]{:S(2)}) copy-start(f32[31,256]{1,0:T(8,128)} %taps.1) | copy-start | bytes 95236
  87.8 54.2 %copy-start.6 = (f32[256]{0:T(256)S(1)}, f32[256]{0:T(256)}, u32[]{:S(2)}) copy-start(f32[256]{0:T(256)} %param.25) | copy-start | bytes 3076
  87.8 54.2 %copy-start.7 = (f32[256]{0:T(256)S(1)}, f32[256]{0:T(256)}, u32[]{:S(2)}) copy-start(f32[256]{0:T(256)} %param.26) | copy-start | bytes 3076
  107.5 52.9 %collective-permute-start.17 = (bf16[272,1024]{1,0:T(8,128)(2,1)}, bf16[272,1024]{1,0:T(8,128)(2,1)S(1)}, u32[]{:S(2)}, u32[]{:S(2)}) collective-permute-start(bf16[272,1024]{1,0:T(8,128)(2,1)} %get-tuple-element.61), channel_id=1, source_target_pairs={{0,16},{4,68},{8,24},{12,76},{16,0},{20,84},{24,8},{28,92},{32,48}... | collective-permute-start | bytes 1671176 | tf_op jit(solution)/shard_map/ppermute | solution.py:41
  110.5 49.9 %collective-permute-start.15 = (bf16[272,1024]{1,0:T(8,128)(2,1)}, bf16[272,1024]{1,0:T(8,128)(2,1)S(1)}, u32[]{:S(2)}, u32[]{:S(2)}) collective-permute-start(bf16[272,1024]{1,0:T(8,128)(2,1)} %get-tuple-element.59), channel_id=1, source_target_pairs={{0,24},{4,100},{8,0},{12,108},{16,8},{20,116},{24,16},{28,124},{32... | collective-permute-start | bytes 1671176 | tf_op jit(solution)/shard_map/ppermute | solution.py:41
  118.6 41.8 %collective-permute-start.16 = (bf16[272,1024]{1,0:T(8,128)(2,1)}, bf16[272,1024]{1,0:T(8,128)(2,1)S(1)}, u32[]{:S(2)}, u32[]{:S(2)}) collective-permute-start(bf16[272,1024]{1,0:T(8,128)(2,1)} %get-tuple-element.60), channel_id=1, source_target_pairs={{0,8},{4,36},{8,16},{12,44},{16,24},{20,52},{24,0},{28,60},{32,40}... | collective-permute-start | bytes 1671176 | tf_op jit(solution)/shard_map/ppermute | solution.py:41
  119.2 22.8 %collective-permute-start.14 = (bf16[30,256]{1,0:T(8,128)(2,1)S(1)}, bf16[30,256]{1,0:T(8,128)(2,1)S(1)}, u32[]{:S(2)}, u32[]{:S(2)}) collective-permute-start(bf16[30,256]{1,0:T(8,128)(2,1)S(1)} %slice.11), channel_id=1, source_target_pairs={{0,4},{4,8},{8,12},{12,16},{16,20},{20,24},{24,28},{28,32},{32,36}... | collective-permute-start | bytes 46088 | tf_op jit(solution)/shard_map/ppermute | solution.py:690
  144.8 15.6 %copy-start.3 = (f32[2]{0:T(128)S(1)}, f32[2]{0:T(128)}, u32[]{:S(2)}) copy-start(f32[2]{0:T(128)} %lam.1) | copy-start | bytes 28
  144.8 15.7 %copy-start.4 = (f32[128]{0:T(128)S(1)}, f32[128]{0:T(128)}, u32[]{:S(2)}) copy-start(f32[128]{0:T(128)} %param.23) | copy-start | bytes 1540
  156.9 9.1 %all-to-all-start.1 = ((bf16[4,144,256]{2,1,0:T(8,128)(2,1)}), bf16[4,144,256]{2,1,0:T(8,128)(2,1)S(1)}, u32[]{:S(2)}, u32[]{:S(2)}) async-start(bf16[4,144,256]{2,1,0:T(8,128)(2,1)} %convolve.1), calls=%async_computation.1 | async-start | bytes 589824 | tf_op jit(solution)/shard_map/all_to_all | solution.py:723
  166.1 22.0 %all-to-all-start = ((bf16[8,128,128]{2,1,0:T(8,128)(2,1)}), bf16[8,128,128]{2,1,0:T(8,128)(2,1)S(1)}, u32[]{:S(2)}, u32[]{:S(2)}) async-start(bf16[8,128,128]{2,1,0:T(8,128)(2,1)} %get-tuple-element.62), calls=%async_computation | async-start | bytes 524288 | tf_op jit(solution)/shard_map/all_to_all | solution.py:737
  182.6 4.2 %collective-permute-start.18 = (f32[2,512]{1,0:T(2,128)S(1)}, f32[2,512]{1,0:T(2,128)S(1)}, u32[]{:S(2)}, u32[]{:S(2)}) collective-permute-start(f32[2,512]{1,0:T(2,128)S(1)} %get-tuple-element.65), channel_id=1, source_target_pairs={{0,100},{4,96},{8,108},{12,104},{16,116},{20,112},{24,124},{28,120... | collective-permute-start | bytes 12296 | tf_op jit(solution)/shard_map/ppermute | solution.py:53

commit v2 on v1

--- a/solution.py
+++ b/solution.py
@@ -105,6 +105,14 @@
     gj = lax.broadcasted_iota(jnp.int32, (256, 256), 1) // 64
     groups = jnp.where(gi == gj, 1.0 / 64, 0.0).astype(BF)
 
+    spread = lax.broadcasted_iota(jnp.int32, (64, 256), 0)
+    spread = (spread == lax.rem(lax.broadcasted_iota(jnp.int32, (64, 256), 1), 64)).astype(BF)
+    rows = [
+        jnp.dot(part.astype(BF), spread, preferred_element_type=F32) for part in split3(qkg[...])
+    ]
+    rows = rows[0] + rows[1] + rows[2]
+    gains = jnp.where(lax.rem(lane // 64, 2) == 0, rows[0:1], rows[1:2])
+
     def table(ref):
         v = jnp.concatenate([ref[pl.ds(at, 128), :] for at in ats], axis=0)
         return jnp.concatenate([v, v], axis=1)
@@ -123,7 +131,7 @@
         ms = jnp.dot(hi, groups, preferred_element_type=F32) + jnp.dot(
             lo, groups, preferred_element_type=F32
         )
-        v = v * lax.rsqrt(ms + 1e-06) * qkg[...]
+        v = v * lax.rsqrt(ms + 1e-06) * gains
         swapped = jnp.where(first, pltpu.roll(v, 256 - 32, 1), pltpu.roll(v, 32, 1))
         return v * cc + swapped * ss
 
@@ -140,7 +148,7 @@
             other[row : row + 128, rows] = (part.T if flip else part).astype(BF)
 
     wq, wk, wv, wa, wg = ws
-    put(0, turned(wq) * (LOG2E / 8.0), True)
+    put(0, turned(wq) * 0.125, True)
     put(128, turned(wk), False)
     put(256, times(wv), True)
     g = times(wa) * jax.nn.sigmoid(times(wg))
@@ -149,10 +157,10 @@
 
 
 def project_first(
-    pos, t0, a1, b1, b2, a2, gain, wq, wk, wv, wa, wg, qkg, cos, sin, mine, gated, other, normed
+    pos, t0, t1, a1, b1, b2, a2, gain, wq, wk, wv, wa, wg, qkg, cos, sin, mine, gated, other, normed
 ):
     project_body(
-        pos, ((t0, 0), (a1, 3), (b1, 3), (b2, 1), (a2, 1)), gain, (wq, wk, wv, wa, wg), qkg, cos,
+        pos, ((t0, 0), (t1, 0), (a1, 3), (b1, 3), (b2, 1), (a2, 1)), gain, (wq, wk, wv, wa, wg), qkg, cos,
         sin, mine, other, gated, normed,
     )
 
@@ -216,15 +224,16 @@
 
 
 def conv_kernel_body(gated, halo, taps, scale, shift, out, ext):
-    ext[0:32, :] = jnp.zeros((32, 256), F32)
-    ext[544:560, :] = jnp.zeros((16, 256), F32)
-    ext[2:32, :] = halo[...].astype(F32)
-    ext[32:544, :] = gated[...].astype(F32)
-    for lanes in (slice(0, 128), slice(128, 256)):
+    for h in range(2):
+        lanes = slice(h * 128, (h + 1) * 128)
+        ext[h, 0:32, :] = jnp.zeros((32, 128), F32)
+        ext[h, 544:560, :] = jnp.zeros((16, 128), F32)
+        ext[h, 2:32, :] = halo[:, lanes].astype(F32)
+        ext[h, 32:544, :] = gated[:, lanes].astype(F32)
         for i in range(4):
             acc = jnp.zeros((128, 128), F32)
             for r in range(8):
-                moved = ext[i * 128 + r : i * 128 + r + 160, lanes]
+                moved = ext[h, i * 128 + r : i * 128 + r + 160, :]
                 for a in range(5):
                     j = a * 8 + r - 2
                     if 0 <= j < 31:
@@ -242,7 +251,7 @@
         out_shape=jax.ShapeDtypeStruct((4, 144, 256), BF),
         in_specs=[vmem()] * 5,
         out_specs=vmem(),
-        scratch_shapes=[pltpu.VMEM((560, 256), F32)],
+        scratch_shapes=[pltpu.VMEM((2, 560, 128), F32)],
         compiler_params=pltpu.CompilerParams(vmem_limit_bytes=4 * 1024 * 1024),
         cost_estimate=pl.CostEstimate(flops=1000000000, bytes_accessed=800000, transcendentals=0),
         name="convolve",
@@ -307,7 +316,7 @@
 
 def weigh(tacc, mref, r, cols, scores, masked):
     n, w = scores.shape
-    s3 = scores.reshape(n // 8, 8, w)
+    s3 = scores.reshape(n // 8, 8, w) * LOG2E
     if mref is not None:
         s3 = s3 - mref[r, :, cols][None]
     p = jnp.exp2(s3).reshape(n, w)
@@ -381,7 +390,8 @@
 
     for s in sources:
         for r in range(4 * s, 4 * s + 4):
-            mref[r] = jnp.broadcast_to(jnp.max(tacc[r], axis=0, keepdims=True), (8, 512))
+            top = jnp.max(tacc[r], axis=0, keepdims=True) * LOG2E
+            mref[r] = jnp.broadcast_to(top, (8, 512))
 
 
 def finish(sources, fast, pos, qz, kvs, kscr, vscr, sbuf, pbuf, oacc, tacc, mref, todo, flag):
@@ -670,20 +680,21 @@
     sine = jnp.sin(angles)
     cos = jnp.concatenate([cosine] * 4, axis=1)
     sin = jnp.concatenate([-sine, sine, -sine, sine], axis=1)
-    qkg = jnp.tile(qk_gain.reshape(1, 128), (1, 2))
-    t0, *weights = prefetch(
-        (tokens, query_weight, key_weight, value_weight, glu_value_weight, glu_gate_weight),
+    weights = prefetch(
+        (query_weight, key_weight, value_weight, glu_value_weight, glu_gate_weight),
         cos,
         sin,
     )
     shared = (
         norm_gain[None, :],
         *weights,
-        qkg,
+        qk_gain,
         cos,
         sin,
     )
-    mine, gated, given = project(project_first, 384, pos, (t0, a1, b1, b2, a2), shared, ())
+    mine, gated, given = project(
+        project_first, 384, pos, (upper, lower, a1, b1, b2, a2), shared, ()
+    )
     near_in = to_mirror(given)
     mine, gated, given = project(project_last, 128, pos, (f1, f2), shared, (mine, gated))
     far_in = to_mirror(given)

time: 192 us -> 190 us (0.990)
  local copies, waits for them, and re-layouts: 4.72 us -> 1.71 us
  waiting for transfers between devices: 19.1 us -> 21.6 us
    ppermute x6, waiting for transfers between devices: 4.06 us -> 6.89 us  [along_x(): lax.ppermute(value, 'tp', [(i, (i + step) % count) for i in range(count)])]
    unnamed x17 -> x15, local copies, waits for them, and re-layouts: 2.88 us -> 0.64 us
  transfers between devices with their start and end apart: 21 -> 21, of which waited for: 8 -> 8; matrix products, arithmetic and copies ran while one was open for 2% -> 1% of each run, Pallas kernels for 34% -> 34%
where the time goes in v2:
time: 190 us
  Pallas kernels  87.5 us (46%)
  starting transfers between devices  76.7 us (40%)
  waiting for transfers between devices  21.6 us (11%)
    pallas_call x5, Pallas kernels, attention_call(): pl.pallas_call(body, out_shape=(*sums, *outs), in_specs=[smem()] + [vmem(...  67.8 us
    ppermute x1, starting transfers between devices, per_device_steps(): lax.ppermute(gated[482:], 'sp', [(i, i + 1) for i in range(NZ * NY * NC -...  22 us
    all_to_all x1, starting transfers between devices, per_device_steps(): lax.all_to_all(packed, ('sp', 'tp'), split_axis=0, concat_axis=0, axis_in...  16.7 us
    ppermute x6, starting transfers between devices, send_query(): lax.ppermute(value, 'sp', moves(lambda z, y, c: (*stepped(z, y, c == 0, s...  14.3 us
    ppermute x6, starting transfers between devices, along_x(): lax.ppermute(value, 'tp', [(i, (i + step) % count) for i in range(count)])  8.74 us
    ppermute x3, waiting for transfers between devices, to_mirror(): lax.ppermute(value, 'sp', moves(lambda z, y, c: (NZ - 1 - z, y, 1 - c)))  7.01 us
    ppermute x6, waiting for transfers between devices, along_x(): lax.ppermute(value, 'tp', [(i, (i + step) % count) for i in range(count)])  6.89 us
    ppermute x3, starting transfers between devices, to_mirror(): lax.ppermute(value, 'sp', moves(lambda z, y, c: (NZ - 1 - z, y, 1 - c)))  6.71 us
  transfers between devices with their start and end apart: 21, of which 8 were waited for; matrix products, arithmetic and copies ran while one was open for 1% of the time, Pallas kernels for 34%

profile of v2, /device:TPU:1, one launch (start us, length us, event | category | flops | bytes accessed | tf_op | source)
XLA Modules:
  0.0 190.1 jit_solution(11171774730302836569)
XLA Ops:
  0.6 1.1 fusion.1
  1.7 0.0 copy-start
  1.7 0.0 copy-start.1
  1.7 3.4 %collective-permute-start.2 = (bf16[64,2048]{1,0:T(8,128)(2,1)S(1)}, bf16[64,2048]{1,0:T(8,128)(2,1)S(1)}, u32[]{:S(2)}, u32[]{:S(2)}) collective-permute-start(bf16[64,2048]{1,0:T(8,128)(2,1)S(1)} %get-tuple-element.68.t1), channel_id=1, source_target_pairs={{0,3},{1,0},{2,1},{3,2},{4,7},{5,4},{6,5},{7,6},{8,11},{9,8},{10,9... | collective-permute-start | bytes 786440 | tf_op jit(solution)/shard_map/ppermute | solution.py:58
  5.1 0.0 collective-permute-start.4
  5.1 0.2 collective-permute-start
  5.3 2.5 %collective-permute-start.5 = (bf16[64,2048]{1,0:T(8,128)(2,1)S(1)}, bf16[64,2048]{1,0:T(8,128)(2,1)S(1)}, u32[]{:S(2)}, u32[]{:S(2)}) collective-permute-start(bf16[64,2048]{1,0:T(8,128)(2,1)S(1)} %get-tuple-element.69.t0), channel_id=1, source_target_pairs={{0,3},{1,0},{2,1},{3,2},{4,7},{5,4},{6,5},{7,6},{8,11},{9,8},{10,9... | collective-permute-start | bytes 786440 | tf_op jit(solution)/shard_map/ppermute | solution.py:58
  7.8 1.0 fusion
  8.8 0.5 pad_maximum_fusion
  9.3 2.5 %prefetch.1 = (bf16[2048,256]{1,0:T(8,128)(2,1)S(1)}, bf16[2048,256]{1,0:T(8,128)(2,1)S(1)}, bf16[2048,256]{1,0:T(8,128)(2,1)S(1)}, bf16[2048,256]{1,0:T(8,128)(2,1)S(1)}, bf16[2048,256]{1,0:T(8,128)(2,1)S(1)}) custom-call(bf16[2048,256]{1,0:T(8,128)(2,1)} %refs_0_.1, bf16[2048,256]{1,0:T(8,128)(2,1)} %refs_1_.1, bf16[2048,256]{1,0:T(8,128)(2,1)} %refs_2_.1, ...), custom_call_target="tpu_custom_call" | custom-call | flops 2000000 | bytes 12000000 | tf_op jit(solution)/shard_map/prefetch/pallas_call | solution.py:77
  11.9 0.1 pad_add_fusion.pos
  11.9 6.9 %collective-permute-done.a1 = bf16[64,2048]{1,0:T(8,128)(2,1)S(1)} collective-permute-done((bf16[64,2048]{1,0:T(8,128)(2,1)S(1)}, bf16[64,2048]{1,0:T(8,128)(2,1)S(1)}, u32[]{:S(2)}, u32[]{:S(2)}) %collective-permute-start) | collective-permute-done | bytes 262176 | tf_op jit(solution)/shard_map/ppermute | solution.py:58
  18.8 0.0 collective-permute-start.1
  18.8 0.0 collective-permute-done.2.a2
  18.8 2.7 %collective-permute-start.3 = (bf16[64,2048]{1,0:T(8,128)(2,1)S(1)}, bf16[64,2048]{1,0:T(8,128)(2,1)S(1)}, u32[]{:S(2)}, u32[]{:S(2)}) collective-permute-start(bf16[64,2048]{1,0:T(8,128)(2,1)S(1)} %collective-permute-done.2.a2), channel_id=1, source_target_pairs={{0,3},{1,0},{2,1},{3,2},{4,7},{5,4},{6,5},{7,6},{8,11},{9,8},{10,9... | collective-permute-start | bytes 786440 | tf_op jit(solution)/shard_map/ppermute | solution.py:58
  21.5 0.0 collective-permute-done.4.b1
  21.5 0.0 collective-permute-done.5.b2
  21.5 4.4 %shard_map.149 = (bf16[384,512]{1,0:T(8,128)(2,1)S(1)}, bf16[512,256]{1,0:T(8,128)(2,1)S(1)}, bf16[384,384]{1,0:T(8,128)(2,1)S(1)}) custom-call(s32[4]{0:T(128)S(1)} %pad_add_fusion.pos, bf16[64,2048]{1,0:T(8,128)(2,1)S(1)} %get-tuple-element.69.t0, bf16[64,2048]{1,0:T(8,128)(2,1)S(1)} %get-tuple-element.68.t1, ...), custom_call_target="tpu_custom_call" | custom-call | flops 2013265920 | bytes 8000000 | tf_op jit(solution)/shard_map/pallas_call | solution.py:181
  25.9 6.1 %collective-permute-start.6 = (bf16[384,384]{1,0:T(8,128)(2,1)S(1)}, bf16[384,384]{1,0:T(8,128)(2,1)S(1)}, u32[]{:S(2)}, u32[]{:S(2)}) collective-permute-start(bf16[384,384]{1,0:T(8,128)(2,1)S(1)} %get-tuple-element.41), channel_id=1, source_target_pairs={{0,100},{4,96},{8,108},{12,104},{16,116},{20,112},{24,124},{28,120... | collective-permute-start | bytes 884744 | tf_op jit(solution)/shard_map/ppermute | solution.py:53
  32.0 0.0 collective-permute-done.1.f1
  32.0 0.0 collective-permute-done.3.f2
  32.0 2.2 %shard_map.150 = (bf16[384,512]{1,0:T(8,128)(2,1)S(1)}, bf16[512,256]{1,0:T(8,128)(2,1)S(1)}, bf16[384,128]{1,0:T(8,128)(2,1)S(1)}) custom-call(s32[4]{0:T(128)S(1)} %pad_add_fusion.pos, bf16[64,2048]{1,0:T(8,128)(2,1)S(1)} %collective-permute-done.1.f1, ...), custom_call_target="tpu_custom_call", output_to_operand_aliasing={{0}: (12, {}), {1}: (13, {})} | custom-call | flops 671088640 | bytes 8000000 | tf_op jit(solution)/shard_map/pallas_call | solution.py:181
  34.2 0.5 collective-permute-start.7
  34.7 4.6 %collective-permute-done.6.near = bf16[384,384]{1,0:T(8,128)(2,1)S(1)} collective-permute-done((bf16[384,384]{1,0:T(8,128)(2,1)S(1)}, bf16[384,384]{1,0:T(8,128)(2,1)S(1)}, u32[]{:S(2)}, u32[]{:S(2)}) %collective-permute-start.6) | collective-permute-done | bytes 294944 | tf_op jit(solution)/shard_map/ppermute | solution.py:53
  39.3 1.1 collective-permute-done.7.far
  40.3 0.7 assemble.1
  41.0 1.4 collective-permute-start.8
  42.4 1.5 collective-permute-start.9
  43.9 0.4 collective-permute-start.12
  44.3 2.3 %collective-permute-start.13 = (bf16[128,1024]{1,0:T(8,128)(2,1)S(1)}, bf16[128,1024]{1,0:T(8,128)(2,1)S(1)}, u32[]{:S(2)}, u32[]{:S(2)}) collective-permute-start(bf16[128,1024]{1,0:T(8,128)(2,1)S(1)} %get-tuple-element.43.q0), channel_id=1, source_target_pairs={{0,24},{4,100},{8,0},{12,108},{16,8},{20,116},{24,16},{28,124},{32... | collective-permute-start | bytes 786440 | tf_op jit(solution)/shard_map/ppermute | solution.py:41
  46.6 1.6 collective-permute-start.10
  48.1 2.4 %shard_map.151 = (f32[16,128,512]{2,1,0:T(8,128)S(1)}, f32[16,8,512]{2,1,0:T(8,128)S(1)}) custom-call(s32[4]{0:T(128)S(1)} %pad_add_fusion.pos, bf16[128,1024]{1,0:T(8,128)(2,1)S(1)} %get-tuple-element.43.q0, bf16[256,1024]{1,0:T(8,128)(2,1)S(1)} %get-tuple-element.44.kv0), custom_call_target="tpu_custom_call" | custom-call | flops 800000000 | bytes 4000000 | tf_op jit(solution)/shard_map/pallas_call | solution.py:529
  50.5 2.9 %collective-permute-done.12.q1 = bf16[128,1024]{1,0:T(8,128)(2,1)S(1)} collective-permute-done((bf16[128,1024]{1,0:T(8,128)(2,1)S(1)}, bf16[128,1024]{1,0:T(8,128)(2,1)S(1)}, u32[]{:S(2)}, u32[]{:S(2)}) %collective-permute-start.12) | collective-permute-done | bytes 262176 | tf_op jit(solution)/shard_map/ppermute | solution.py:41
  53.4 0.0 collective-permute-start.11
  53.4 0.0 collective-permute-done.13.q2
  53.4 0.0 collective-permute-done.8.kv1
  53.4 0.0 collective-permute-done.9.kv2
  53.4 9.0 %shard_map.152 = (f32[16,128,512]{2,1,0:T(8,128)S(1)}, f32[16,8,512]{2,1,0:T(8,128)S(1)}) custom-call(s32[4]{0:T(128)S(1)} %pad_add_fusion.pos, bf16[128,1024]{1,0:T(8,128)(2,1)S(1)} %get-tuple-element.43.q0, bf16[128,1024]{1,0:T(8,128)(2,1)S(1)} %collective-permute-done.12.q1, ...), custom_call_target="tpu_custom_call", output_to_operand_aliasing={{0}: (7, {}), {1}: (8, {})} | custom-call | flops 6400000000 | bytes 4000000 | tf_op jit(solution)/shard_map/pallas_call | solution.py:529
  62.5 0.0 collective-permute-done.10.kv3
  62.5 24.4 %shard_map.153 = (f32[16,128,512]{2,1,0:T(8,128)S(1)}, f32[16,8,512]{2,1,0:T(8,128)S(1)}, bf16[272,1024]{1,0:T(8,128)(2,1)}, bf16[272,1024]{1,0:T(8,128)(2,1)}) custom-call(s32[4]{0:T(128)S(1)} %pad_add_fusion.pos, bf16[128,1024]{1,0:T(8,128)(2,1)S(1)} %collective-permute-done.12.q1, ...), custom_call_target="tpu_custom_call", output_to_operand_aliasing={{0}: (7, {}), {1}: (8, {})} | custom-call | flops 1600000000 | bytes 4000000 | tf_op jit(solution)/shard_map/pallas_call | solution.py:529
  86.9 0.0 collective-permute-done.11.q3
  86.9 0.0 copy-start.6
  86.9 19.7 %shard_map.154 = (f32[16,128,512]{2,1,0:T(8,128)S(1)}, f32[16,8,512]{2,1,0:T(8,128)S(1)}, bf16[272,1024]{1,0:T(8,128)(2,1)}) custom-call(s32[4]{0:T(128)S(1)} %pad_add_fusion.pos, bf16[128,1024]{1,0:T(8,128)(2,1)S(1)} %collective-permute-done.11.q3, bf16[256,1024]{1,0:T(8,128)(2,1)S(1)} %get-tuple-element.44.kv0, ...), custom_call_target="tpu_custom_call", output_to_operand_aliasing={{0}: (6, {}), {1}: (7, {})} | custom-call | flops 3200000000 | bytes 4000000 | tf_op jit(solution)/shard_map/pallas_call | solution.py:529
  106.6 3.0 %collective-permute-start.17 = (bf16[272,1024]{1,0:T(8,128)(2,1)}, bf16[272,1024]{1,0:T(8,128)(2,1)S(1)}, u32[]{:S(2)}, u32[]{:S(2)}) collective-permute-start(bf16[272,1024]{1,0:T(8,128)(2,1)} %get-tuple-element.59), channel_id=1, source_target_pairs={{0,16},{4,68},{8,24},{12,76},{16,0},{20,84},{24,8},{28,92},{32,48}... | collective-permute-start | bytes 1671176 | tf_op jit(solution)/shard_map/ppermute | solution.py:41
  109.5 8.1 %collective-permute-start.15 = (bf16[272,1024]{1,0:T(8,128)(2,1)}, bf16[272,1024]{1,0:T(8,128)(2,1)S(1)}, u32[]{:S(2)}, u32[]{:S(2)}) collective-permute-start(bf16[272,1024]{1,0:T(8,128)(2,1)} %get-tuple-element.57), channel_id=1, source_target_pairs={{0,24},{4,100},{8,0},{12,108},{16,8},{20,116},{24,16},{28,124},{32... | collective-permute-start | bytes 1671176 | tf_op jit(solution)/shard_map/ppermute | solution.py:41
  117.7 0.6 collective-permute-start.16
  118.2 22.0 %collective-permute-start.14 = (bf16[30,256]{1,0:T(8,128)(2,1)S(1)}, bf16[30,256]{1,0:T(8,128)(2,1)S(1)}, u32[]{:S(2)}, u32[]{:S(2)}) collective-permute-start(bf16[30,256]{1,0:T(8,128)(2,1)S(1)} %slice.11), channel_id=1, source_target_pairs={{0,4},{4,8},{8,12},{12,16},{16,20},{20,24},{24,28},{28,32},{32,36}... | collective-permute-start | bytes 46088 | tf_op jit(solution)/shard_map/ppermute | solution.py:701
  140.3 0.8 collective-permute-done.14.halo
  141.2 1.8 convolve.1
  143.0 12.2 %shard_map.155 = (f32[4,128,512]{2,1,0:T(8,128)S(1)}, f32[8,1024]{1,0:T(8,128)S(1)}) custom-call(s32[4]{0:T(128)S(1)} %pad_add_fusion.pos, bf16[128,1024]{1,0:T(8,128)(2,1)S(1)} %get-tuple-element.43.q0, bf16[256,1024]{1,0:T(8,128)(2,1)S(1)} %get-tuple-element.44.kv0, bf16[256,1024]{1,0:T(8,128)(2,1)S(1)} %collective-permute-done.8.kv1, ...), custom_call_target="tpu_custom_call" | custom-call | flops 800000000 | bytes 4000000 | tf_op jit(solution)/shard_map/pallas_call | solution.py:529
  155.2 3.7 %all-to-all-start.1 = ((bf16[4,144,256]{2,1,0:T(8,128)(2,1)}), bf16[4,144,256]{2,1,0:T(8,128)(2,1)S(1)}, u32[]{:S(2)}, u32[]{:S(2)}) async-start(bf16[4,144,256]{2,1,0:T(8,128)(2,1)} %convolve.1), calls=%async_computation.1 | async-start | bytes 589824 | tf_op jit(solution)/shard_map/all_to_all | solution.py:734
  158.9 0.0 collective-permute-done.17.r3
  158.9 0.0 collective-permute-done.15.r1
  158.9 0.0 collective-permute-done.16.r2
  158.9 0.0 copy-done.2
  159.0 2.2 %merge.1 = (bf16[8,128,128]{2,1,0:T(8,128)(2,1)}, f32[2,512]{1,0:T(2,128)S(1)}, f32[2,512]{1,0:T(2,128)S(1)}) custom-call(s32[4]{0:T(128)S(1)} %pad_add_fusion.pos, f32[2]{0:T(128)S(1)} %copy-done.2, f32[4,128,512]{2,1,0:T(8,128)S(1)} %get-tuple-element.53.own, f32[8,1024]{1,0:T(8,128)S(1)} %get-tuple-element.56.stats, ...), custom_call_target="tpu_custom_call" | custom-call | flops 500000000 | bytes 4000000 | tf_op jit(solution)/shard_map/merge/pallas_call | solution.py:582
  161.1 3.2 %all-to-all-done.1.moved = bf16[4,144,256]{2,1,0:T(8,128)(2,1)S(1)} async-done(((bf16[4,144,256]{2,1,0:T(8,128)(2,1)}), bf16[4,144,256]{2,1,0:T(8,128)(2,1)S(1)}, u32[]{:S(2)}, u32[]{:S(2)}) %all-to-all-start.1) | async-done | bytes 294944 | tf_op jit(solution)/shard_map/all_to_all | solution.py:734
  164.4 16.7 %all-to-all-start = ((bf16[8,128,128]{2,1,0:T(8,128)(2,1)}), bf16[8,128,128]{2,1,0:T(8,128)(2,1)S(1)}, u32[]{:S(2)}, u32[]{:S(2)}) async-start(bf16[8,128,128]{2,1,0:T(8,128)(2,1)} %get-tuple-element.60), calls=%async_computation | async-start | bytes 524288 | tf_op jit(solution)/shard_map/all_to_all | solution.py:748
  181.1 0.2 collective-permute-start.18
  181.2 2.7 %shard_map.156.part = f32[128,2048]{1,0:T(8,128)S(1)} custom-call(bf16[4,144,256]{2,1,0:T(8,128)(2,1)S(1)} %all-to-all-done.1.moved, f32[2,512]{1,0:T(2,128)S(1)} %get-tuple-element.62.token, bf16[2048,2048]{1,0:T(8,128)(2,1)} %w.3), custom_call_target="tpu_custom_call" | custom-call | flops 600000000 | bytes 5000000 | tf_op jit(solution)/shard_map/pallas_call | solution.py:646
  184.0 1.4 collective-permute-done.18
  185.3 0.6 copy.26
  185.9 0.7 all-to-all-done.moved
  186.6 3.3 %shard_map.157 = bf16[128,2048]{1,0:T(8,128)(2,1)} custom-call(bf16[8,128,128]{2,1,0:T(8,128)(2,1)S(1)} %all-to-all-done.moved, f32[128,2048]{1,0:T(8,128)S(1)} %shard_map.156.part, bf16[2048,2048]{1,0:T(8,128)(2,1)} %w.3), custom_call_target="tpu_custom_call" | custom-call | flops 600000000 | bytes 5000000 | tf_op jit(solution)/shard_map/pallas_call | solution.py:646
  (14 shorter events, 0.0 us)
Async XLA Ops:
  1.7 19.8 %copy-start = (f32[2048]{0:T(1024)S(1)}, f32[2048]{0:T(1024)}, u32[]{:S(2)}) copy-start(f32[2048]{0:T(1024)} %param.15) | copy-start | bytes 24580
  1.7 19.8 %copy-start.1 = (f32[2,64]{1,0:T(2,128)S(1)}, f32[2,64]{1,0:T(2,128)}, u32[]{:S(2)}) copy-start(f32[2,64]{1,0:T(2,128)} %qkg.3) | copy-start | bytes 1540
  1.7 17.1 %collective-permute-start.2 = (bf16[64,2048]{1,0:T(8,128)(2,1)S(1)}, bf16[64,2048]{1,0:T(8,128)(2,1)S(1)}, u32[]{:S(2)}, u32[]{:S(2)}) collective-permute-start(bf16[64,2048]{1,0:T(8,128)(2,1)S(1)} %get-tuple-element.68.t1), channel_id=1, source_target_pairs={{0,3},{1,0},{2,1},{3,2},{4,7},{5,4},{6,5},{7,6},{8,11},{9,8},{10,9... | collective-permute-start | bytes 786440 | tf_op jit(solution)/shard_map/ppermute | solution.py:58
  5.1 16.4 %collective-permute-start.4 = (bf16[64,2048]{1,0:T(8,128)(2,1)S(1)}, bf16[64,2048]{1,0:T(8,128)(2,1)S(1)}, u32[]{:S(2)}, u32[]{:S(2)}) collective-permute-start(bf16[64,2048]{1,0:T(8,128)(2,1)S(1)} %get-tuple-element.68.t1), channel_id=1, source_target_pairs={{0,1},{1,2},{2,3},{3,0},{4,5},{5,6},{6,7},{7,4},{8,9},{9,10},{10,1... | collective-permute-start | bytes 786440 | tf_op jit(solution)/shard_map/ppermute | solution.py:58
  5.1 13.7 %collective-permute-start = (bf16[64,2048]{1,0:T(8,128)(2,1)S(1)}, bf16[64,2048]{1,0:T(8,128)(2,1)S(1)}, u32[]{:S(2)}, u32[]{:S(2)}) collective-permute-start(bf16[64,2048]{1,0:T(8,128)(2,1)S(1)} %get-tuple-element.69.t0), channel_id=1, source_target_pairs={{0,1},{1,2},{2,3},{3,0},{4,5},{5,6},{6,7},{7,4},{8,9},{9,10},{10,1... | collective-permute-start | bytes 786440 | tf_op jit(solution)/shard_map/ppermute | solution.py:58
  5.3 16.2 %collective-permute-start.5 = (bf16[64,2048]{1,0:T(8,128)(2,1)S(1)}, bf16[64,2048]{1,0:T(8,128)(2,1)S(1)}, u32[]{:S(2)}, u32[]{:S(2)}) collective-permute-start(bf16[64,2048]{1,0:T(8,128)(2,1)S(1)} %get-tuple-element.69.t0), channel_id=1, source_target_pairs={{0,3},{1,0},{2,1},{3,2},{4,7},{5,4},{6,5},{7,6},{8,11},{9,8},{10,9... | collective-permute-start | bytes 786440 | tf_op jit(solution)/shard_map/ppermute | solution.py:58
  18.8 13.2 %collective-permute-start.1 = (bf16[64,2048]{1,0:T(8,128)(2,1)S(1)}, bf16[64,2048]{1,0:T(8,128)(2,1)S(1)}, u32[]{:S(2)}, u32[]{:S(2)}) collective-permute-start(bf16[64,2048]{1,0:T(8,128)(2,1)S(1)} %collective-permute-done.a1), channel_id=1, source_target_pairs={{0,1},{1,2},{2,3},{3,0},{4,5},{5,6},{6,7},{7,4},{8,9},{9,10},{10,1... | collective-permute-start | bytes 786440 | tf_op jit(solution)/shard_map/ppermute | solution.py:58
  18.8 13.2 %collective-permute-start.3 = (bf16[64,2048]{1,0:T(8,128)(2,1)S(1)}, bf16[64,2048]{1,0:T(8,128)(2,1)S(1)}, u32[]{:S(2)}, u32[]{:S(2)}) collective-permute-start(bf16[64,2048]{1,0:T(8,128)(2,1)S(1)} %collective-permute-done.2.a2), channel_id=1, source_target_pairs={{0,3},{1,0},{2,1},{3,2},{4,7},{5,4},{6,5},{7,6},{8,11},{9,8},{10,9... | collective-permute-start | bytes 786440 | tf_op jit(solution)/shard_map/ppermute | solution.py:58
  25.9 13.3 %collective-permute-start.6 = (bf16[384,384]{1,0:T(8,128)(2,1)S(1)}, bf16[384,384]{1,0:T(8,128)(2,1)S(1)}, u32[]{:S(2)}, u32[]{:S(2)}) collective-permute-start(bf16[384,384]{1,0:T(8,128)(2,1)S(1)} %get-tuple-element.41), channel_id=1, source_target_pairs={{0,100},{4,96},{8,108},{12,104},{16,116},{20,112},{24,124},{28,120... | collective-permute-start | bytes 884744 | tf_op jit(solution)/shard_map/ppermute | solution.py:53
  34.2 6.1 %collective-permute-start.7 = (bf16[384,128]{1,0:T(8,128)(2,1)S(1)}, bf16[384,128]{1,0:T(8,128)(2,1)S(1)}, u32[]{:S(2)}, u32[]{:S(2)}) collective-permute-start(bf16[384,128]{1,0:T(8,128)(2,1)S(1)} %get-tuple-element.42), channel_id=1, source_target_pairs={{0,100},{4,96},{8,108},{12,104},{16,116},{20,112},{24,124},{28,120... | collective-permute-start | bytes 294920 | tf_op jit(solution)/shard_map/ppermute | solution.py:53
  41.0 12.4 %collective-permute-start.8 = (bf16[256,1024]{1,0:T(8,128)(2,1)S(1)}, bf16[256,1024]{1,0:T(8,128)(2,1)S(1)}, u32[]{:S(2)}, u32[]{:S(2)}) collective-permute-start(bf16[256,1024]{1,0:T(8,128)(2,1)S(1)} %get-tuple-element.44.kv0), channel_id=1, source_target_pairs={{0,32},{4,12},{8,40},{12,20},{16,48},{20,28},{24,56},{28,4},{32,64... | collective-permute-start | bytes 1572872 | tf_op jit(solution)/shard_map/ppermute | solution.py:47
  42.4 11.1 %collective-permute-start.9 = (bf16[256,1024]{1,0:T(8,128)(2,1)S(1)}, bf16[256,1024]{1,0:T(8,128)(2,1)S(1)}, u32[]{:S(2)}, u32[]{:S(2)}) collective-permute-start(bf16[256,1024]{1,0:T(8,128)(2,1)S(1)} %get-tuple-element.44.kv0), channel_id=1, source_target_pairs={{0,96},{4,28},{8,104},{12,4},{16,112},{20,12},{24,120},{28,20},{32... | collective-permute-start | bytes 1572872 | tf_op jit(solution)/shard_map/ppermute | solution.py:47
  43.9 9.5 %collective-permute-start.12 = (bf16[128,1024]{1,0:T(8,128)(2,1)S(1)}, bf16[128,1024]{1,0:T(8,128)(2,1)S(1)}, u32[]{:S(2)}, u32[]{:S(2)}) collective-permute-start(bf16[128,1024]{1,0:T(8,128)(2,1)S(1)} %get-tuple-element.43.q0), channel_id=1, source_target_pairs={{0,8},{4,36},{8,16},{12,44},{16,24},{20,52},{24,0},{28,60},{32,40}... | collective-permute-start | bytes 786440 | tf_op jit(solution)/shard_map/ppermute | solution.py:41
  44.3 9.1 %collective-permute-start.13 = (bf16[128,1024]{1,0:T(8,128)(2,1)S(1)}, bf16[128,1024]{1,0:T(8,128)(2,1)S(1)}, u32[]{:S(2)}, u32[]{:S(2)}) collective-permute-start(bf16[128,1024]{1,0:T(8,128)(2,1)S(1)} %get-tuple-element.43.q0), channel_id=1, source_target_pairs={{0,24},{4,100},{8,0},{12,108},{16,8},{20,116},{24,16},{28,124},{32... | collective-permute-start | bytes 786440 | tf_op jit(solution)/shard_map/ppermute | solution.py:41
  46.6 15.9 %collective-permute-start.10 = (bf16[256,1024]{1,0:T(8,128)(2,1)S(1)}, bf16[256,1024]{1,0:T(8,128)(2,1)S(1)}, u32[]{:S(2)}, u32[]{:S(2)}) collective-permute-start(bf16[256,1024]{1,0:T(8,128)(2,1)S(1)} %get-tuple-element.44.kv0), channel_id=1, source_target_pairs={{0,64},{4,20},{8,72},{12,28},{16,80},{20,4},{24,88},{28,12},{32,96... | collective-permute-start | bytes 1572872 | tf_op jit(solution)/shard_map/ppermute | solution.py:47
  53.4 33.5 %collective-permute-start.11 = (bf16[128,1024]{1,0:T(8,128)(2,1)S(1)}, bf16[128,1024]{1,0:T(8,128)(2,1)S(1)}, u32[]{:S(2)}, u32[]{:S(2)}) collective-permute-start(bf16[128,1024]{1,0:T(8,128)(2,1)S(1)} %get-tuple-element.43.q0), channel_id=1, source_target_pairs={{0,16},{4,68},{8,24},{12,76},{16,0},{20,84},{24,8},{28,92},{32,48}... | collective-permute-start | bytes 786440 | tf_op jit(solution)/shard_map/ppermute | solution.py:41
  86.9 54.3 %copy-start.4 = (f32[31,256]{1,0:T(8,128)S(1)}, f32[31,256]{1,0:T(8,128)}, u32[]{:S(2)}) copy-start(f32[31,256]{1,0:T(8,128)} %taps.1) | copy-start | bytes 95236
  86.9 54.3 %copy-start.5 = (f32[256]{0:T(256)S(1)}, f32[256]{0:T(256)}, u32[]{:S(2)}) copy-start(f32[256]{0:T(256)} %param.25) | copy-start | bytes 3076
  86.9 54.3 %copy-start.6 = (f32[256]{0:T(256)S(1)}, f32[256]{0:T(256)}, u32[]{:S(2)}) copy-start(f32[256]{0:T(256)} %param.26) | copy-start | bytes 3076
  106.6 52.3 %collective-permute-start.17 = (bf16[272,1024]{1,0:T(8,128)(2,1)}, bf16[272,1024]{1,0:T(8,128)(2,1)S(1)}, u32[]{:S(2)}, u32[]{:S(2)}) collective-permute-start(bf16[272,1024]{1,0:T(8,128)(2,1)} %get-tuple-element.59), channel_id=1, source_target_pairs={{0,16},{4,68},{8,24},{12,76},{16,0},{20,84},{24,8},{28,92},{32,48}... | collective-permute-start | bytes 1671176 | tf_op jit(solution)/shard_map/ppermute | solution.py:41
  109.5 49.4 %collective-permute-start.15 = (bf16[272,1024]{1,0:T(8,128)(2,1)}, bf16[272,1024]{1,0:T(8,128)(2,1)S(1)}, u32[]{:S(2)}, u32[]{:S(2)}) collective-permute-start(bf16[272,1024]{1,0:T(8,128)(2,1)} %get-tuple-element.57), channel_id=1, source_target_pairs={{0,24},{4,100},{8,0},{12,108},{16,8},{20,116},{24,16},{28,124},{32... | collective-permute-start | bytes 1671176 | tf_op jit(solution)/shard_map/ppermute | solution.py:41
  117.7 41.3 %collective-permute-start.16 = (bf16[272,1024]{1,0:T(8,128)(2,1)}, bf16[272,1024]{1,0:T(8,128)(2,1)S(1)}, u32[]{:S(2)}, u32[]{:S(2)}) collective-permute-start(bf16[272,1024]{1,0:T(8,128)(2,1)} %get-tuple-element.58), channel_id=1, source_target_pairs={{0,8},{4,36},{8,16},{12,44},{16,24},{20,52},{24,0},{28,60},{32,40}... | collective-permute-start | bytes 1671176 | tf_op jit(solution)/shard_map/ppermute | solution.py:41
  118.2 22.9 %collective-permute-start.14 = (bf16[30,256]{1,0:T(8,128)(2,1)S(1)}, bf16[30,256]{1,0:T(8,128)(2,1)S(1)}, u32[]{:S(2)}, u32[]{:S(2)}) collective-permute-start(bf16[30,256]{1,0:T(8,128)(2,1)S(1)} %slice.11), channel_id=1, source_target_pairs={{0,4},{4,8},{8,12},{12,16},{16,20},{20,24},{24,28},{28,32},{32,36}... | collective-permute-start | bytes 46088 | tf_op jit(solution)/shard_map/ppermute | solution.py:701
  143.0 16.0 %copy-start.2 = (f32[2]{0:T(128)S(1)}, f32[2]{0:T(128)}, u32[]{:S(2)}) copy-start(f32[2]{0:T(128)} %lam.1) | copy-start | bytes 28
  143.0 16.0 %copy-start.3 = (f32[128]{0:T(128)S(1)}, f32[128]{0:T(128)}, u32[]{:S(2)}) copy-start(f32[128]{0:T(128)} %param.23) | copy-start | bytes 1540
  155.2 9.1 %all-to-all-start.1 = ((bf16[4,144,256]{2,1,0:T(8,128)(2,1)}), bf16[4,144,256]{2,1,0:T(8,128)(2,1)S(1)}, u32[]{:S(2)}, u32[]{:S(2)}) async-start(bf16[4,144,256]{2,1,0:T(8,128)(2,1)} %convolve.1), calls=%async_computation.1 | async-start | bytes 589824 | tf_op jit(solution)/shard_map/all_to_all | solution.py:734
  164.4 22.2 %all-to-all-start = ((bf16[8,128,128]{2,1,0:T(8,128)(2,1)}), bf16[8,128,128]{2,1,0:T(8,128)(2,1)S(1)}, u32[]{:S(2)}, u32[]{:S(2)}) async-start(bf16[8,128,128]{2,1,0:T(8,128)(2,1)} %get-tuple-element.60), calls=%async_computation | async-start | bytes 524288 | tf_op jit(solution)/shard_map/all_to_all | solution.py:748
  181.1 4.2 %collective-permute-start.18 = (f32[2,512]{1,0:T(2,128)S(1)}, f32[2,512]{1,0:T(2,128)S(1)}, u32[]{:S(2)}, u32[]{:S(2)}) collective-permute-start(f32[2,512]{1,0:T(2,128)S(1)} %get-tuple-element.63), channel_id=1, source_target_pairs={{0,100},{4,96},{8,108},{12,104},{16,116},{20,112},{24,124},{28,120... | collective-permute-start | bytes 12296 | tf_op jit(solution)/shard_map/ppermute | solution.py:53
